TPU v7x, 32 devices: a whole 2x2x4 slice. The times are simulated.
32 devices in a mesh: ep: 8 (over z, core), tp: 4 (over y, x).
Axes of the slice: x: 2, y: 2, z: 4, core: 2. Of those that a mesh axis runs over, the one named last changes fastest.
Arguments:
- queries: bfloat16 [1024, 1536], P('ep', 'tp'), may hold values from -64 to 64
- kv_latent: bfloat16 [1024, 512], P('ep'), may hold values from -60 to 60
- rope_key: bfloat16 [1024, 32], P('ep'), may hold values from -64 to 64
- latent_gain: float32 [512], replicated, may hold values from 0.1 to 1.9
- key_up: bfloat16 [512, 1024], P(None, 'tp'), may hold values from -0.25 to 0.25
- value_up: bfloat16 [512, 1024], P(None, 'tp'), may hold values from -40 to 40
- query_gain: float32 [96], replicated, may hold values from 0.3 to 4
- key_gain: float32 [96], replicated, may hold values from 0.3 to 4
- out_gain: float32 [1024], replicated, may hold values from 0.1 to 1.9
- out_proj: bfloat16 [1024, 4096], P(None, 'tp'), may hold values from -0.1875 to 0.1875
- moe_input: bfloat16 [1024, 4096], P('ep'), may hold values from -60 to 60
- moe_gain: float32 [4096], replicated, may hold values from 0.1 to 1.9
- expert_ids: int32 [1024, 2], P('ep'), may hold values from 0 to 31, as said below
- route_weights: float32 [1024, 2], P('ep'), may hold values from 0.2 to 1
- w_gate: bfloat16 [32, 4096, 2048], P('ep', None, 'tp'), may hold values from -0.09375 to 0.09375
- w_up: bfloat16 [32, 4096, 2048], P('ep', None, 'tp'), may hold values from -0.09375 to 0.09375
- w_down: bfloat16 [32, 2048, 4096], P('ep', 'tp'), may hold values from -0.125 to 0.125
Outputs:
- mixed: bfloat16 [1024, 4096], P('ep', 'tp')
- expert_out: bfloat16 [1024, 4096], P('ep', 'tp')
Inputs may be any that keep to these rules, and one draw needn't show every extreme that they name: `expert_ids`: both experts of a row lie in one group (g * 8 to g * 8 + 7) and differ. In each aligned block of 128 rows no expert is named more than 12 times, and some expert is named exactly 12 times.
All inputs are finite; a program needn't handle non-finite values.
Results may differ from a plain program's by a relative error of at most 0.015.
The roundings to bfloat16 on the way count: a program that leaves them out, or rounds other values in their place, can miss the bound.
Values may be sent and summed in bfloat16 or wider, within the bound.
A program may use at most 128 MiB of HBM per device.

v0:
```python
import functools

import jax
import jax.numpy as jnp
from jax import lax
from jax.experimental import pallas as pl
from jax.experimental.pallas import tpu as pltpu
from jax.sharding import PartitionSpec as P

NOPE = 64
ROPE = 32
VDIM = 64
QKD = 96
CAP = 12


EPS = 1e-06
THETA = 10000.0


def rotate_half(values_in, positions):
    half_width = ROPE // 2
    inverse = THETA ** (-jnp.arange(half_width, dtype=jnp.float32) / half_width)
    angles = positions.astype(jnp.float32)[:, None] * inverse
    cosine = jnp.cos(angles)[:, None, :]
    sine = jnp.sin(angles)[:, None, :]
    first_half = values_in[..., :half_width]
    second_half = values_in[..., half_width:]
    return jnp.concatenate(
        [first_half * cosine - second_half * sine, second_half * cosine + first_half * sine],
        axis=-1,
    )


def head_norm(values_in, gain_vec):
    return (
        values_in
        * lax.rsqrt(jnp.mean(values_in * values_in, axis=-1, keepdims=True) + EPS)
        * gain_vec
    )


def make_queries(queries, query_gain, positions):
    row_count = queries.shape[0]
    head_count = queries.shape[1] // QKD
    normed = head_norm(queries.astype(jnp.float32).reshape(row_count, head_count, QKD), query_gain)
    turned = jnp.concatenate(
        [normed[..., :NOPE], rotate_half(normed[..., NOPE:], positions)], axis=-1
    )
    return turned.astype(jnp.bfloat16)


def make_keys(latent, rope_part, latent_gain, key_up, value_up, key_gain, positions):
    row_count = latent.shape[0]
    head_count = key_up.shape[1] // NOPE
    latent_f = latent.astype(jnp.float32)
    latent_n = (
        latent_f
        * lax.rsqrt(jnp.mean(latent_f * latent_f, axis=-1, keepdims=True) + EPS)
        * latent_gain
    ).astype(jnp.bfloat16)
    key_nope = jnp.dot(latent_n, key_up, preferred_element_type=jnp.float32).astype(jnp.bfloat16)
    key_nope = lax.optimization_barrier(key_nope)
    value_rows = jnp.dot(latent_n, value_up, preferred_element_type=jnp.float32).astype(
        jnp.bfloat16
    )
    shared = jnp.broadcast_to(
        rope_part.astype(jnp.float32)[:, None, :], (row_count, head_count, ROPE)
    )
    key_full = jnp.concatenate(
        [key_nope.astype(jnp.float32).reshape(row_count, head_count, NOPE), shared], axis=-1
    )
    normed = head_norm(key_full, key_gain)
    turned = jnp.concatenate(
        [normed[..., :NOPE], rotate_half(normed[..., NOPE:], positions)], axis=-1
    )
    return (turned.astype(jnp.bfloat16), value_rows.reshape(row_count, head_count, VDIM))


def shards(
    queries,
    kv_latent,
    rope_key,
    latent_gain,
    key_up,
    value_up,
    query_gain,
    key_gain,
    out_gain,
    out_proj,
    moe_input,
    moe_gain,
    expert_ids,
    route_weights,
    w_gate,
    w_up,
    w_down,
):
    tok_rows = queries.shape[0]
    head_count = key_up.shape[1] // NOPE
    query_pos = lax.axis_index("ep") * tok_rows + jnp.arange(tok_rows, dtype=jnp.int32)
    query_rot = make_queries(queries, query_gain, query_pos)
    inv_scale = QKD ** (-0.5)
    blocks_in = (
        lax.all_gather(kv_latent, "ep", axis=0, tiled=True),
        lax.all_gather(rope_key, "ep", axis=0, tiled=True),
    )
    key_pos = jnp.arange(blocks_in[0].shape[0], dtype=jnp.int32)
    key_rot, value_rows = make_keys(
        blocks_in[0], blocks_in[1], latent_gain, key_up, value_up, key_gain, key_pos
    )
    top_prev = jnp.full((head_count, tok_rows), -1e30, jnp.float32)
    key_pos = jnp.arange(key_rot.shape[0], dtype=jnp.int32)
    scores = (
        jnp.einsum("qhd,khd->hqk", query_rot, key_rot, preferred_element_type=jnp.float32)
        * inv_scale
    )
    visible = key_pos[None, :] <= query_pos[:, None]
    scores = jnp.where(visible[None], scores, -1e30)
    top_new = jnp.maximum(top_prev, jnp.max(scores, axis=-1))
    expo = jnp.exp(scores - top_new[..., None])
    total_new = jnp.sum(expo, axis=-1)
    accum_new = jnp.einsum(
        "hqk,khd->hqd", expo.astype(jnp.bfloat16), value_rows, preferred_element_type=jnp.float32
    )
    attn = (accum_new / total_new[..., None]).astype(jnp.bfloat16)
    attn = attn.transpose(1, 0, 2).reshape(tok_rows, head_count * VDIM)
    block_f = lax.all_gather(attn, "tp", axis=1, tiled=True).astype(jnp.float32)
    scaled = (block_f * out_gain[None, :]).astype(jnp.bfloat16)
    product = jnp.dot(scaled, out_proj, preferred_element_type=jnp.float32)
    product, squares = (product, jnp.sum(block_f * block_f, axis=-1))
    mixed = (product * lax.rsqrt(squares / out_gain.shape[0] + EPS)[:, None]).astype(jnp.bfloat16)
    row_count = moe_input.shape[0]
    top_count = expert_ids.shape[1]
    local_experts = w_gate.shape[0]
    ep_count = lax.axis_size("ep")
    expert_count = local_experts * ep_count
    stream_f = moe_input.astype(jnp.float32)
    normed = (
        stream_f * lax.rsqrt(jnp.mean(stream_f * stream_f, axis=-1, keepdims=True) + EPS) * moe_gain
    ).astype(jnp.bfloat16)
    flat_ids = expert_ids.reshape(-1)
    onehot = (flat_ids[:, None] == jnp.arange(expert_count, dtype=jnp.int32)[None, :]).astype(
        jnp.int32
    )
    slot_rank = jnp.sum((jnp.cumsum(onehot, axis=0) - onehot) * onehot, axis=1)
    slot_index = flat_ids * CAP + slot_rank
    token_index = jnp.arange(row_count * top_count, dtype=jnp.int32) // top_count
    slot_token = jnp.zeros((expert_count * CAP,), jnp.int32).at[slot_index].set(token_index)
    slot_used = jnp.zeros((expert_count * CAP,), jnp.bool_).at[slot_index].set(True)
    outgoing = jnp.where(slot_used[:, None], normed[slot_token], jnp.zeros((), jnp.bfloat16))
    outgoing = outgoing.reshape(ep_count, local_experts, CAP, normed.shape[1])
    piece_width = normed.shape[1] // lax.axis_size("tp")
    my_columns = lax.dynamic_slice_in_dim(
        outgoing, lax.axis_index("tp") * piece_width, piece_width, 3
    )
    arrived_part = lax.all_to_all(my_columns, "ep", split_axis=0, concat_axis=0, tiled=True)
    piece = lax.all_gather(arrived_part, "tp", axis=3, tiled=True)
    gate_acc = jnp.einsum("secd,edf->secf", piece, w_gate, preferred_element_type=jnp.float32)
    upper_acc = jnp.einsum("secd,edf->secf", piece, w_up, preferred_element_type=jnp.float32)
    hidden = (jax.nn.silu(gate_acc) * upper_acc).astype(jnp.bfloat16)
    out_cols = w_down.shape[2] // lax.axis_size("tp")
    term = jnp.einsum("secf,efd->dsec", hidden, w_down, preferred_element_type=jnp.float32)
    summed = lax.psum_scatter(
        term.reshape(lax.axis_size("tp") * out_cols, -1).astype(jnp.bfloat16),
        "tp",
        scatter_dimension=0,
        tiled=True,
    )
    expert_y = summed.T.reshape(ep_count, local_experts * CAP, out_cols)
    returned_rows = lax.all_to_all(expert_y, "ep", split_axis=0, concat_axis=0, tiled=True).reshape(
        expert_count * CAP, out_cols
    )
    picked = returned_rows[slot_index].reshape(row_count, top_count, out_cols).astype(jnp.float32)
    expert_out = jnp.sum(picked * route_weights[..., None], axis=1).astype(jnp.bfloat16)
    return (mixed, expert_out)


MESH = pl.DeviceIdType.MESH
GROUP = 8
PAD = 128


def group_cap():
    return GROUP * CAP // 2


def rdma(src, dst, send_sem, recv_sem, device):
    copy = pltpu.make_async_remote_copy(
        src_ref=src,
        dst_ref=dst,
        send_sem=send_sem,
        recv_sem=recv_sem,
        device_id=device,
        device_id_type=MESH,
    )
    copy.start()
    return copy


def arrived(dst, sem, device):
    pltpu.make_async_remote_copy(
        src_ref=dst,
        dst_ref=dst,
        send_sem=sem,
        recv_sem=sem,
        device_id=device,
        device_id_type=MESH,
    ).wait_recv()


def places(planes):
    ep = lax.axis_index("ep")
    tp = lax.axis_index("tp")
    plane = ep // 2
    core = ep % 2

    def along(offset):
        return (lax.rem(plane + offset + planes, planes) * 2 + core, tp)

    partner = (plane * 2 + 1 - core, tp)
    near_x = (ep, tp ^ 1)
    near_y = (ep, tp ^ 2)
    corner = (ep, tp ^ 3)
    return tp, along, partner, near_x, near_y, corner


def greet(peers):
    barrier = pltpu.get_barrier_semaphore()
    for peer in peers:
        pl.semaphore_signal(barrier, inc=1, device_id=peer, device_id_type=MESH)
    pl.semaphore_wait(barrier, len(peers))


def routed_kernel(
    planes,
    out_ref,
    meta_ref,
    kv_ref,
    gate_ref,
    up_ref,
    down_ref,
    part_ref,
    keys_ref,
    rows_ref,
    metas_ref,
    gates,
    ups,
    downs,
    taken,
    given,
    ws,
    zs,
    zr,
    xs,
    xr,
    ps,
    pr,
    loc,
):
    tp, along, partner, near_x, near_y, _ = places(planes)
    greet([along(d) for d in range(1, planes)] + [partner, near_x, near_y])
    half_w = out_ref.shape[2] // 2
    half_r = kv_ref.shape[0] // 2
    sent = []
    local = [
        pltpu.make_async_copy(kv_ref, keys_ref.at[tp, 0, 0], loc.at[0]),
        pltpu.make_async_copy(meta_ref.at[0], metas_ref.at[0, 0], loc.at[1]),
        pltpu.make_async_copy(out_ref.at[0], rows_ref.at[tp, 0, 0], loc.at[2]),
    ]
    for copy in local:
        copy.start()
    order = sorted(range(1, planes), key=lambda d: (min(d, planes - d), d))
    for d in order:
        sent.append(
            rdma(meta_ref.at[d], metas_ref.at[0, d], zs.at[1, d], zr.at[1, d], along(d))
        )
        sent.append(
            rdma(out_ref.at[d], rows_ref.at[tp, 0, d], zs.at[2, d], zr.at[2, d], along(d))
        )
    for d in order:
        sent.append(rdma(kv_ref, keys_ref.at[tp, 0, d], zs.at[0, d], zr.at[0, d], along(d)))
    experts = gate_ref.shape[0]
    down_slots = downs.shape[0]

    def fetch(which, source, target, expert):
        return pltpu.make_async_copy(source, target, ws.at[which, expert])

    gate_in = [fetch(0, gate_ref.at[e], gates.at[e], e) for e in range(experts)]
    up_in = [fetch(1, up_ref.at[e], ups.at[e], e) for e in range(experts)]
    down_in = [fetch(2, down_ref.at[e], downs.at[e % down_slots], e) for e in range(experts)]
    for e in range(experts):
        gate_in[e].start()
        up_in[e].start()
        if e < down_slots:
            down_in[e].start()
    for copy in local:
        copy.wait()
    bufs = (keys_ref, rows_ref)

    def halves(kind, ref):
        if kind == 0:
            return ref.at[pl.ds(0, half_r)], ref.at[pl.ds(half_r, half_r)]
        return ref.at[:, pl.ds(0, half_w)], ref.at[:, pl.ds(half_w, half_w)]

    def to_partner(kind, which, q, d):
        sent.append(
            rdma(
                bufs[kind].at[q, 0, d],
                bufs[kind].at[q, 1, d],
                ps.at[kind, which, d],
                pr.at[kind, which, d],
                partner,
            )
        )

    def first(kind, d):
        mine = bufs[kind].at[tp, 0, d]
        if d > 0:
            arrived(mine, zr.at[2 * kind, d], along(-d))
        sent.append(rdma(mine, mine, xs.at[kind, 0, d], xr.at[kind, 0, d], near_x))
        sent.append(rdma(mine, mine, xs.at[kind, 1, d], xr.at[kind, 1, d], near_y))
        to_partner(kind, 0, tp, d)
        if kind == 1:
            part = metas_ref.at[0, d]
            if d > 0:
                arrived(part, zr.at[1, d], along(-d))
            sent.append(rdma(part, metas_ref.at[1, d], ps.at[2, 0, d], pr.at[2, 0, d], partner))

    def second(kind, d):
        from_x = bufs[kind].at[tp ^ 1, 0, d]
        arrived(from_x, xr.at[kind, 0, d], near_x)
        low, _ = halves(kind, from_x)
        sent.append(rdma(low, low, xs.at[kind, 2, d], xr.at[kind, 2, d], near_y))
        from_y = bufs[kind].at[tp ^ 2, 0, d]
        arrived(from_y, xr.at[kind, 1, d], near_y)
        _, high = halves(kind, from_y)
        sent.append(rdma(high, high, xs.at[kind, 3, d], xr.at[kind, 3, d], near_x))
        to_partner(kind, 1, tp ^ 1, d)
        to_partner(kind, 2, tp ^ 2, d)

    def third(kind, d):
        low, high = halves(kind, bufs[kind].at[tp ^ 3, 0, d])
        arrived(low, xr.at[kind, 2, d], near_y)
        arrived(high, xr.at[kind, 3, d], near_x)
        to_partner(kind, 3, tp ^ 3, d)

    jobs = [(1, 0), (0, 0)] + [(1, d) for d in order] + [(0, d) for d in order]
    for step in range(len(jobs) + 4):
        if step < len(jobs):
            first(*jobs[step])
        if 0 <= step - 2 < len(jobs):
            second(*jobs[step - 2])
        if 0 <= step - 4 < len(jobs):
            third(*jobs[step - 4])
    for d in range(planes):
        for kind in range(2):
            for which, flip in enumerate((0, 1, 2, 3)):
                arrived(bufs[kind].at[tp ^ flip, 1, d], pr.at[kind, which, d], partner)
        arrived(metas_ref.at[1, d], pr.at[2, 0, d], partner)

    f32, bf = jnp.float32, jnp.bfloat16
    core = lax.axis_index("ep") % 2
    parts, width = part_ref.shape[1], part_ref.shape[3]
    cap = out_ref.shape[1]
    blocks = 2 * planes
    row_total, slots = blocks * cap, blocks * CAP
    info = metas_ref[...].reshape(row_total, PAD)
    codes = info.astype(f32)
    block_of = lax.broadcasted_iota(jnp.int32, (blocks, cap, 1), 0).reshape(row_total, 1)
    slot_ids = lax.broadcasted_iota(jnp.int32, (row_total, experts * slots), 1)
    match = []
    for pick in range(2):
        code = codes[:, pick : pick + 1].astype(jnp.int32) - 1 - core * (experts * CAP)
        inside = (codes[:, pick : pick + 1] > 0.5) & (code >= 0) & (code < experts * CAP)
        expert = jnp.zeros_like(code)
        for e in range(1, experts):
            expert += (code >= e * CAP).astype(jnp.int32)
        where = expert * (slots - CAP) + block_of * CAP + code
        match.append((slot_ids == jnp.where(inside, where, -1)).astype(f32).astype(bf))
    place = match[0] + match[1]
    turned = (((0,), (0,)), ((), ()))
    weights = jnp.zeros((experts * slots, 1), f32)
    for pick in range(2):
        found = lax.dot_general(match[pick], info, turned, preferred_element_type=f32)
        weights += found[:, 2 + pick : 3 + pick] + found[:, 4 + pick : 5 + pick]
    for q in range(parts):
        rows = rows_ref[q].reshape(row_total, width)
        taken[:, q * width : (q + 1) * width] = lax.dot_general(
            place, rows, turned, preferred_element_type=f32
        ).astype(bf)
    for e in range(experts):
        first_slot = e * slots
        picked = taken[first_slot : first_slot + slots, :]
        gate_in[e].wait()
        gate = jnp.dot(picked, gates[e], preferred_element_type=f32)
        up_in[e].wait()
        upper = jnp.dot(picked, ups[e], preferred_element_type=f32)
        hidden = (
            gate / (1.0 + jnp.exp(-gate)) * upper * weights[first_slot : first_slot + slots]
        ).astype(bf)
        down_in[e].wait()
        for q in range(parts):
            given[first_slot : first_slot + slots, q * width : (q + 1) * width] = jnp.dot(
                hidden,
                downs[e % down_slots, :, q * width : (q + 1) * width],
                preferred_element_type=f32,
            ).astype(bf)
        if e + down_slots < experts:
            down_in[e + down_slots].start()
    for q in range(parts):
        back = jnp.dot(
            place, given[:, q * width : (q + 1) * width], preferred_element_type=f32
        )
        part_ref[:, q] = back.astype(bf).reshape(blocks, cap, width)
    for copy in sent:
        copy.wait_send()


def routed(outgoing, metas, kv_part, w_gate, w_up, w_down, tp_count):
    planes, cap, width = outgoing.shape
    experts, model, hidden = w_gate.shape
    blocks = 2 * planes
    slot_total = experts * blocks * CAP
    dma = pltpu.SemaphoreType.DMA
    bf = jnp.bfloat16
    vmem = pl.BlockSpec(memory_space=pltpu.VMEM)
    hbm = pl.BlockSpec(memory_space=pl.ANY)
    return pl.pallas_call(
        functools.partial(routed_kernel, planes),
        out_shape=(
            jax.ShapeDtypeStruct((blocks, tp_count, cap, width), bf),
            jax.ShapeDtypeStruct((tp_count, 2, planes) + kv_part.shape, bf),
        ),
        in_specs=[vmem] * 3 + [hbm] * 3,
        out_specs=(vmem,) * 2,
        scratch_shapes=[
            pltpu.VMEM((tp_count, 2, planes, cap, width), bf),
            pltpu.VMEM((2, planes, cap, PAD), bf),
            pltpu.VMEM((experts, model, hidden), bf),
            pltpu.VMEM((experts, model, hidden), bf),
            pltpu.VMEM((2, hidden, model), bf),
            pltpu.VMEM((slot_total, model), bf),
            pltpu.VMEM((slot_total, model), bf),
            dma((3, experts)),
            dma((3, planes)),
            dma((3, planes)),
            dma((2, 4, planes)),
            dma((2, 4, planes)),
            dma((3, 4, planes)),
            dma((3, 4, planes)),
            dma((3,)),
        ],
        compiler_params=pltpu.CompilerParams(
            collective_id=0, has_side_effects=True, vmem_limit_bytes=67043328
        ),
        name="routed",
    )(outgoing, metas, kv_part, w_gate, w_up, w_down)


def combine_kernel(
    planes,
    part_ref,
    attn_ref,
    back_ref,
    heads_ref,
    other,
    sums,
    bx1,
    by1,
    bx2,
    by2,
    done,
    as_,
    ar,
    ps,
    pr,
    xs,
    xr,
    zs,
    zr,
    loc,
):
    tp, along, partner, near_x, near_y, corner = places(planes)
    greet([along(d) for d in range(1, planes)] + [partner, near_x, near_y, corner])
    half_w = part_ref.shape[4] // 2
    low, high = pl.ds(0, half_w), pl.ds(half_w, half_w)
    sent = []
    order = list(range(1, planes)) + [0]
    for d in order:
        sent.append(rdma(part_ref.at[1, d], other.at[d], ps.at[d], pr.at[d], partner))
    own = pltpu.make_async_copy(attn_ref, heads_ref.at[tp], loc.at[0])
    own.start()
    for i, peer in enumerate((near_x, near_y, corner)):
        sent.append(rdma(attn_ref, heads_ref.at[tp], as_.at[i], ar.at[i], peer))

    def first(d):
        arrived(other.at[d], pr.at[d], partner)
        for q in range(part_ref.shape[2]):
            sums[d, q] = (
                part_ref[0, d, q].astype(jnp.float32) + other[d, q].astype(jnp.float32)
            ).astype(jnp.bfloat16)
        piece = sums.at[d, tp ^ 3]
        sent.append(rdma(piece.at[:, low], bx1.at[d], xs.at[0, d], xr.at[0, d], near_x))
        sent.append(rdma(piece.at[:, high], by1.at[d], xs.at[1, d], xr.at[1, d], near_y))

    def second(d):
        arrived(bx1.at[d], xr.at[0, d], near_x)
        sums[d, tp ^ 2, :, low] = (
            sums[d, tp ^ 2, :, low].astype(jnp.float32) + bx1[d].astype(jnp.float32)
        ).astype(jnp.bfloat16)
        sent.append(rdma(sums.at[d, tp ^ 2], by2.at[d], xs.at[3, d], xr.at[3, d], near_y))
        arrived(by1.at[d], xr.at[1, d], near_y)
        sums[d, tp ^ 1, :, high] = (
            sums[d, tp ^ 1, :, high].astype(jnp.float32) + by1[d].astype(jnp.float32)
        ).astype(jnp.bfloat16)
        sent.append(rdma(sums.at[d, tp ^ 1], bx2.at[d], xs.at[2, d], xr.at[2, d], near_x))

    def third(d):
        arrived(bx2.at[d], xr.at[2, d], near_x)
        arrived(by2.at[d], xr.at[3, d], near_y)
        full = (
            sums[d, tp].astype(jnp.float32)
            + bx2[d].astype(jnp.float32)
            + by2[d].astype(jnp.float32)
        ).astype(jnp.bfloat16)
        if d == 0:
            back_ref[0] = full
        else:
            done[d] = full
            sent.append(rdma(done.at[d], back_ref.at[d], zs.at[d], zr.at[d], along(-d)))

    for step in range(planes + 2):
        if step < planes:
            first(order[step])
        if 0 <= step - 1 < planes:
            second(order[step - 1])
        if 0 <= step - 2 < planes:
            third(order[step - 2])
    own.wait()
    for i, peer in enumerate((near_x, near_y, corner)):
        arrived(heads_ref.at[tp ^ (i + 1)], ar.at[i], peer)
    for d in range(1, planes):
        arrived(back_ref.at[d], zr.at[d], along(d))
    for copy in sent:
        copy.wait_send()


def combine(parts, attn):
    _, planes, tp_count, cap, width = parts.shape
    dma = pltpu.SemaphoreType.DMA
    bf = jnp.bfloat16
    return pl.pallas_call(
        functools.partial(combine_kernel, planes),
        out_shape=(
            jax.ShapeDtypeStruct((planes, cap, width), bf),
            jax.ShapeDtypeStruct((tp_count,) + attn.shape, bf),
        ),
        in_specs=[pl.BlockSpec(memory_space=pltpu.VMEM)] * 2,
        out_specs=(pl.BlockSpec(memory_space=pltpu.VMEM),) * 2,
        scratch_shapes=[
            pltpu.VMEM((planes, tp_count, cap, width), bf),
            pltpu.VMEM((planes, tp_count, cap, width), bf),
            pltpu.VMEM((planes, cap, width // 2), bf),
            pltpu.VMEM((planes, cap, width // 2), bf),
            pltpu.VMEM((planes, cap, width), bf),
            pltpu.VMEM((planes, cap, width), bf),
            pltpu.VMEM((planes, cap, width), bf),
            dma((3,)),
            dma((3,)),
            dma((planes,)),
            dma((planes,)),
            dma((4, planes)),
            dma((4, planes)),
            dma((planes,)),
            dma((planes,)),
            dma((1,)),
        ],
        compiler_params=pltpu.CompilerParams(
            collective_id=1, has_side_effects=True, vmem_limit_bytes=40 * 2**20
        ),
        name="combine",
    )(parts, attn)


def grouped_shards(
    queries,
    kv_latent,
    rope_key,
    latent_gain,
    key_up,
    value_up,
    query_gain,
    key_gain,
    out_gain,
    out_proj,
    moe_input,
    moe_gain,
    expert_ids,
    route_weights,
    w_gate,
    w_up,
    w_down,
):
    f32, bf = jnp.float32, jnp.bfloat16
    ep, tp = lax.axis_index("ep"), lax.axis_index("tp")
    tp_count = lax.axis_size("tp")
    planes = lax.axis_size("ep") // 2
    plane, core = ep // 2, ep % 2
    tokens, model = moe_input.shape
    width = model // tp_count
    cap = group_cap()

    group = expert_ids[:, 0] // GROUP
    offset = lax.rem(group - plane + planes, planes)
    before = (jnp.arange(tokens)[:, None] > jnp.arange(tokens)[None, :]).astype(bf)
    in_group = offset[:, None] == jnp.arange(planes)[None, :]
    local_ids = expert_ids % GROUP
    hit = [offset[:, None] * GROUP + local_ids[:, k : k + 1] == jnp.arange(planes * GROUP)[None, :] for k in range(2)]
    counted = jnp.concatenate([in_group, hit[0] | hit[1]], axis=1).astype(bf)
    earlier = jnp.dot(before, counted, preferred_element_type=f32)
    rank = jnp.sum(jnp.where(in_group, earlier[:, :planes], 0.0), axis=1).astype(jnp.int32)
    codes = [
        local_ids[:, k].astype(f32) * CAP
        + jnp.sum(jnp.where(hit[k], earlier[:, planes:], 0.0), axis=1)
        + 1.0
        for k in range(2)
    ]
    weight_high = lax.reduce_precision(route_weights, 8, 7)
    weight_low = route_weights - weight_high
    meta = jnp.concatenate(
        [codes[0][:, None], codes[1][:, None], weight_high, weight_low], axis=1
    ).astype(bf)
    meta = jnp.pad(meta, ((0, 0), (0, PAD - meta.shape[1])))
    slot = offset * cap + rank
    select = (jnp.arange(planes * cap)[:, None] == slot[None, :]).astype(bf)

    stream_f = moe_input.astype(f32)
    scale = lax.rsqrt(jnp.mean(stream_f * stream_f, axis=-1, keepdims=True) + EPS)
    own_cols = lax.dynamic_slice_in_dim(moe_input, tp * width, width, 1).astype(f32)
    own_gain = lax.dynamic_slice_in_dim(moe_gain, tp * width, width, 0)
    normed = (own_cols * scale * own_gain).astype(bf)
    outgoing = jnp.dot(select, normed, preferred_element_type=f32).astype(bf)
    metas_out = jnp.dot(select, meta, preferred_element_type=f32).astype(bf)

    kv_rows = kv_latent.shape[0] // tp_count
    kv_all = jnp.pad(
        jnp.concatenate([kv_latent, rope_key], axis=1), ((0, 0), (0, PAD - ROPE))
    )
    kv_part = lax.dynamic_slice_in_dim(kv_all, tp * kv_rows, kv_rows, 0)
    partial, keys = routed(
        outgoing.reshape(planes, cap, width),
        metas_out.reshape(planes, cap, PAD),
        kv_part,
        w_gate,
        w_up,
        w_down,
        tp_count,
    )
    partial = partial.reshape(2, planes, tp_count, cap, width)

    tok_rows = queries.shape[0]
    head_count = key_up.shape[1] // NOPE
    query_pos = ep * tok_rows + jnp.arange(tok_rows, dtype=jnp.int32)
    query_rot = make_queries(queries, query_gain, query_pos)
    latent_width = kv_latent.shape[1]
    key_table = keys.reshape(-1, keys.shape[-1])
    quarter = jnp.arange(tp_count, dtype=jnp.int32)[:, None, None, None]
    parity = jnp.arange(2, dtype=jnp.int32)[None, :, None, None]
    away = jnp.arange(planes, dtype=jnp.int32)[None, None, :, None]
    key_block = lax.rem(plane - away + planes, planes) * 2 + lax.rem(core + parity, 2)
    key_pos = (
        key_block * tok_rows
        + quarter * kv_rows
        + jnp.arange(kv_rows, dtype=jnp.int32)[None, None, None, :]
    ).reshape(-1)
    key_rot, value_rows = make_keys(
        key_table[:, :latent_width],
        key_table[:, latent_width : latent_width + ROPE],
        latent_gain,
        key_up,
        value_up,
        key_gain,
        key_pos,
    )
    scores = (
        jnp.einsum("qhd,khd->hqk", query_rot, key_rot, preferred_element_type=f32) * QKD ** (-0.5)
    )
    visible = key_pos[None, :] <= query_pos[:, None]
    scores = jnp.where(visible[None], scores, -1e30)
    expo = jnp.exp(scores - jnp.max(scores, axis=-1, keepdims=True))
    total = jnp.sum(expo, axis=-1)
    accum = jnp.einsum("hqk,khd->hqd", expo.astype(bf), value_rows, preferred_element_type=f32)
    attn = (accum / total[..., None]).astype(bf)
    attn = attn.transpose(1, 0, 2).reshape(tok_rows, head_count * VDIM)

    returned, heads = combine(partial, attn)

    block_f = heads.transpose(1, 0, 2).reshape(tok_rows, -1).astype(f32)
    scaled = (block_f * out_gain[None, :]).astype(bf)
    product = jnp.dot(scaled, out_proj, preferred_element_type=f32)
    squares = jnp.sum(block_f * block_f, axis=-1)
    mixed = (product * lax.rsqrt(squares / out_gain.shape[0] + EPS)[:, None]).astype(bf)
    expert_out = lax.dot_general(
        select,
        returned.reshape(planes * cap, width),
        (((0,), (0,)), ((), ())),
        preferred_element_type=f32,
    ).astype(bf)
    return (mixed, expert_out)


def layer(*arrays):
    local_experts = arrays[14].shape[0]
    fits = lax.axis_size("tp") == 4 and 2 * local_experts == GROUP
    return grouped_shards(*arrays) if fits else shards(*arrays)


def solution(mesh):
    in_specs = (
        P("ep", "tp"),
        P("ep", None),
        P("ep", None),
        P(),
        P(None, "tp"),
        P(None, "tp"),
        P(),
        P(),
        P(),
        P(None, "tp"),
        P("ep", None),
        P(),
        P("ep", None),
        P("ep", None),
        P("ep", None, "tp"),
        P("ep", None, "tp"),
        P("ep", "tp", None),
    )
    out_specs = (P("ep", "tp"), P("ep", "tp"))
    return jax.shard_map(layer, mesh=mesh, in_specs=in_specs, out_specs=out_specs, check_vma=False)
```

profile of v0, /device:TPU:0, one launch (start us, length us, event | category | flops | bytes accessed | tf_op | source)
XLA Modules:
  0.0 99.9 jit_solution(14108931584072933940)
XLA Ops:
  0.7 0.7 dynamic_slice.10
  1.4 1.5 %multiply_reduce_fusion = f32[128]{0:T(128)S(1)} fusion(bf16[128,4096]{1,0:T(8,128)(2,1)} %param.27), kind=kLoop, calls=%fused_computation.7 | loop fusion | flops 1572736 | bytes 1049088 | tf_op jit(solution)/shard_map/reduce_sum | solution.py:639
  2.9 0.7 and_select_fusion
  3.6 0.7 add_bitcast_fusion.1
  4.3 0.1 fusion.37
  4.5 0.7 fusion.65
  5.2 2.1 %convolution_convert_fusion.2 = bf16[192,1024]{1,0:T(8,128)(2,1)} fusion(f32[1024]{0:T(1024)S(1)} %dynamic_slice.10, f32[128]{0:T(128)S(1)} %add_rsqrt_fusion.4, bf16[128,4096]{1,0:T(8,128)(2,1)} %param.27, s32[]{:T(128)S(6)} %select_n.57, s32[128]{0:T(128)S(1)} %fusion.65), kind=kOutput, calls=%fused_computation.16 | convolution fusion | flops 51077120 | bytes 660484 | tf_op jit(solution)/shard_map/dot_general | solution.py:643
  7.3 0.7 reduce-precision_convert_fusion
  8.0 0.8 convolution_convert_fusion.4
  8.8 0.1 copy.30
  8.9 0.6 fusion.41.kv_ref
  9.5 49.8 %routed.1 = (bf16[8,4,48,1024]{3,2,1,0:T(8,128)(2,1)}, bf16[4,2,4,32,640]{4,3,2,1,0:T(8,128)(2,1)}) custom-call(bf16[4,48,1024]{2,1,0:T(8,128)(2,1)} %bitcast.61, bf16[4,48,128]{2,1,0:T(8,128)(2,1)} %bitcast.67, bf16[32,640]{1,0:T(8,128)(2,1)} %fusion.41.kv_ref, bf16[4,4096,512]{2,1,0:T(8,128)(2,1)} %gate_ref.1, bf16[4,4096,512]{2,1,0:T(8,128)(2,1)} %up_ref.1, ...), custom_call_target="tpu_custom_call" | custom-call | tf_op jit(solution)/shard_map/routed/pallas_call | solution.py:429
  59.4 1.6 %fusion = f32[1024]{0:T(1024)S(1)} fusion(bf16[1024,640]{1,0:T(8,128)(2,1)} %bitcast.62), kind=kLoop, calls=%fused_computation.2 | loop fusion | flops 1571840 | bytes 1052672 | tf_op jit(solution)/shard_map/reduce_sum | solution.py:59
  61.0 0.0 copy-start.14
  61.0 2.8 %convolution_convert_fusion = bf16[1024,256]{0,1:T(8,128)(2,1)} fusion(bf16[512,256]{1,0:T(8,128)(2,1)} %param.22, f32[512]{0:T(512)} %param.20, f32[1024]{0:T(1024)S(1)} %add_rsqrt_fusion.1, bf16[1024,640]{1,0:T(8,128)(2,1)} %bitcast.63), kind=kOutput, calls=%fused_computation.14 | convolution fusion | flops 270794752 | bytes 1841152 | tf_op jit(solution)/shard_map/dot_general | solution.py:64
  63.8 0.1 add_multiply_fusion
  63.9 0.1 broadcast_add_fusion
  64.0 0.1 iota_add_fusion
  64.0 0.1 add.247
  64.1 0.1 broadcast_compare_fusion
  64.3 0.1 copy.36
  64.4 0.1 broadcast_in_dim.22
  64.5 0.7 convolution_convert_fusion.1
  65.2 0.2 copy.32
  65.4 0.2 multiply_reduce_fusion.1
  65.6 0.2 copy-done.12
  65.9 0.4 multiply_multiply_fusion
  66.3 0.3 multiply_cosine_fusion
  66.6 0.1 subtract_convert_fusion
  66.7 0.1 slice.98
  66.8 0.0 copy-done.6
  66.8 0.1 copy.31
  66.9 0.1 multiply_multiply_fusion.1
  67.0 0.1 multiply_cosine_fusion.1
  67.2 0.7 fusion.3
  67.9 0.6 fusion.4
  68.5 0.4 copy-done.15
  68.9 0.7 fusion.8
  69.7 0.1 copy.34.attn_ref
  69.8 1.0 %copy-done = bf16[8,4,48,1024]{3,2,1,0:T(8,128)(2,1)S(1)} copy-done((bf16[8,4,48,1024]{3,2,1,0:T(8,128)(2,1)S(1)}, bf16[8,4,48,1024]{3,2,1,0:T(8,128)(2,1)}, u32[]{:S(2)}) %copy-start) | copy-done | bytes 3145752
  70.8 24.6 %combine.1 = (bf16[4,48,1024]{2,1,0:T(8,128)(2,1)S(1)}, bf16[4,128,256]{2,1,0:T(8,128)(2,1)S(1)}) custom-call(bf16[2,4,4,48,1024]{4,3,2,1,0:T(8,128)(2,1)S(1)} %bitcast.55, bf16[128,256]{1,0:T(8,128)(2,1)S(1)} %copy.34.attn_ref), custom_call_target="tpu_custom_call" | custom-call | tf_op jit(solution)/shard_map/combine/pallas_call | solution.py:553
  95.4 0.7 copy-done.1
  96.2 0.2 copy.35
  96.4 0.2 fusion.20
  96.6 0.1 fusion.19
  96.8 1.0 copy-done.3
  97.8 1.2 %fusion.6 = bf16[128,1024]{1,0:T(8,128)(2,1)} fusion(bf16[128,1024]{0,1:T(8,128)(2,1)S(1)} %fusion.20, bf16[1024,1024]{1,0:T(8,128)(2,1)S(1)} %copy-done.3, f32[128]{0:T(128)S(1)} %add_rsqrt_fusion.3), kind=kOutput, calls=%fused_computation.19 | convolution fusion | flops 268697600 | bytes 2621952 | tf_op jit(solution)/shard_map/dot_general | solution.py:701
  98.9 1.0 convolution_convert_fusion.3
  (47 shorter events, 0.3 us)
Async XLA Ops:
  0.6 8.3 %copy-start.5 = (bf16[128,512]{1,0:T(8,128)(2,1)S(1)}, bf16[128,512]{1,0:T(8,128)(2,1)}, u32[]{:S(2)}) copy-start(bf16[128,512]{1,0:T(8,128)(2,1)} %param.18) | copy-start | bytes 393220
  0.6 8.1 %copy-start.7 = (bf16[128,32]{0,1:T(8,128)(2,1)S(1)}, bf16[128,32]{0,1:T(8,128)(2,1)}, u32[]{:S(2)}) copy-start(bf16[128,32]{0,1:T(8,128)(2,1)} %param.19) | copy-start | bytes 24580
  5.2 3.5 %copy-start.8 = (s32[128]{0:T(128)}, s32[128]{0:T(128)S(1)}, u32[]{:S(2)}) copy-start(s32[128]{0:T(128)S(1)} %fusion.65) | copy-start | bytes 1540
  59.4 4.9 %copy-start.4 = (bf16[4,2,4,32,640]{4,3,2,1,0:T(8,128)(2,1)S(1)}, bf16[4,2,4,32,640]{4,3,2,1,0:T(8,128)(2,1)}, u32[]{:S(2)}) copy-start(bf16[4,2,4,32,640]{4,3,2,1,0:T(8,128)(2,1)} %get-tuple-element.7) | copy-start | bytes 3932164
  61.0 3.5 %copy-start.13 = (bf16[512,256]{1,0:T(8,128)(2,1)S(1)}, bf16[512,256]{1,0:T(8,128)(2,1)}, u32[]{:S(2)}) copy-start(bf16[512,256]{1,0:T(8,128)(2,1)} %param.21) | copy-start | bytes 786436
  61.0 3.5 %copy-start.14 = (f32[512]{0:T(512)S(1)}, f32[512]{0:T(512)}, u32[]{:S(2)}) copy-start(f32[512]{0:T(512)} %param.20) | copy-start | bytes 6148
  65.2 0.7 copy-start.12
  65.9 0.9 copy-start.6
  66.3 0.7 copy-start.11
  67.9 1.0 %copy-start.15 = (bf16[1024,256]{0,1:T(8,128)(2,1)S(1)}, bf16[1024,256]{0,1:T(8,128)(2,1)}, u32[]{:S(2)}) copy-start(bf16[1024,256]{0,1:T(8,128)(2,1)} %convolution_convert_fusion) | copy-start | bytes 1572868
  68.9 1.9 %copy-start = (bf16[8,4,48,1024]{3,2,1,0:T(8,128)(2,1)S(1)}, bf16[8,4,48,1024]{3,2,1,0:T(8,128)(2,1)}, u32[]{:S(2)}) copy-start(bf16[8,4,48,1024]{3,2,1,0:T(8,128)(2,1)} %get-tuple-element.6) | copy-start | bytes 9437188
  70.8 25.6 %copy-start.10 = (f32[1024]{0:T(1024)S(1)}, f32[1024]{0:T(1024)}, u32[]{:S(2)}) copy-start(f32[1024]{0:T(1024)} %param.25) | copy-start | bytes 12292
  95.4 0.7 copy-start.1
  96.2 1.6 %copy-start.3 = (bf16[1024,1024]{1,0:T(8,128)(2,1)S(1)}, bf16[1024,1024]{1,0:T(8,128)(2,1)}, u32[]{:S(2)}) copy-start(bf16[1024,1024]{1,0:T(8,128)(2,1)} %param.26) | copy-start | bytes 6291460
  96.4 2.5 %copy-start.2 = (bf16[4,48,1024]{2,1,0:T(8,128)(2,1)S(1)}, bf16[4,48,1024]{2,1,0:T(8,128)(2,1)}, u32[]{:S(2)}) copy-start(bf16[4,48,1024]{2,1,0:T(8,128)(2,1)} %copy-done.1) | copy-start | bytes 1179652
  96.4 2.5 %copy-start.9 = (s32[128]{0:T(128)S(1)}, s32[128]{0:T(128)}, u32[]{:S(2)}) copy-start(s32[128]{0:T(128)} %copy-done.8) | copy-start | bytes 1540
where the time goes:
time: 100 us; the launch traced here: 99.9 us
  Pallas kernels  74.4 us (74%)
  matrix products  9.99 us (10%)
  other arithmetic  9.19 us (9%)
  local copies, waits for them, and re-layouts  5.28 us (5%)
  between operations  1.01 us (1%)
    pallas_call x1, Pallas kernels, routed(): pl.pallas_call(functools.partial(routed_kernel, planes), out_shape=(jax.S...  49.8 us
    pallas_call x1, Pallas kernels, combine(): pl.pallas_call(functools.partial(combine_kernel, planes), out_shape=(jax....  24.6 us
    unnamed x34, local copies, waits for them, and re-layouts  3.72 us
    dot_general x1, matrix products, make_keys(): jnp.dot(latent_n, value_up, preferred_element_type=jnp.float32)  2.77 us
    dot_general x1, matrix products, grouped_shards(): outgoing = jnp.dot(select, normed, preferred_element_type=f32).astype(bf)  2.05 us

commit v1 on v0

v1 whole, which is shorter than its diff:
```python
import functools

import jax
import jax.numpy as jnp
import numpy as np
from jax import lax
from jax.experimental import pallas as pl
from jax.experimental.pallas import tpu as pltpu
from jax.sharding import PartitionSpec as P

NOPE = 64
ROPE = 32
VDIM = 64
QKD = 96
CAP = 12


EPS = 1e-06
THETA = 10000.0


def rotate_half(values_in, positions):
    half_width = ROPE // 2
    inverse = THETA ** (-jnp.arange(half_width, dtype=jnp.float32) / half_width)
    angles = positions.astype(jnp.float32)[:, None] * inverse
    cosine = jnp.cos(angles)[:, None, :]
    sine = jnp.sin(angles)[:, None, :]
    first_half = values_in[..., :half_width]
    second_half = values_in[..., half_width:]
    return jnp.concatenate(
        [first_half * cosine - second_half * sine, second_half * cosine + first_half * sine],
        axis=-1,
    )


def head_norm(values_in, gain_vec):
    return (
        values_in
        * lax.rsqrt(jnp.mean(values_in * values_in, axis=-1, keepdims=True) + EPS)
        * gain_vec
    )


def make_queries(queries, query_gain, positions):
    row_count = queries.shape[0]
    head_count = queries.shape[1] // QKD
    normed = head_norm(queries.astype(jnp.float32).reshape(row_count, head_count, QKD), query_gain)
    turned = jnp.concatenate(
        [normed[..., :NOPE], rotate_half(normed[..., NOPE:], positions)], axis=-1
    )
    return turned.astype(jnp.bfloat16)


def make_keys(latent, rope_part, latent_gain, key_up, value_up, key_gain, positions):
    row_count = latent.shape[0]
    head_count = key_up.shape[1] // NOPE
    latent_f = latent.astype(jnp.float32)
    latent_n = (
        latent_f
        * lax.rsqrt(jnp.mean(latent_f * latent_f, axis=-1, keepdims=True) + EPS)
        * latent_gain
    ).astype(jnp.bfloat16)
    key_nope = jnp.dot(latent_n, key_up, preferred_element_type=jnp.float32).astype(jnp.bfloat16)
    key_nope = lax.optimization_barrier(key_nope)
    value_rows = jnp.dot(latent_n, value_up, preferred_element_type=jnp.float32).astype(
        jnp.bfloat16
    )
    shared = jnp.broadcast_to(
        rope_part.astype(jnp.float32)[:, None, :], (row_count, head_count, ROPE)
    )
    key_full = jnp.concatenate(
        [key_nope.astype(jnp.float32).reshape(row_count, head_count, NOPE), shared], axis=-1
    )
    normed = head_norm(key_full, key_gain)
    turned = jnp.concatenate(
        [normed[..., :NOPE], rotate_half(normed[..., NOPE:], positions)], axis=-1
    )
    return (turned.astype(jnp.bfloat16), value_rows.reshape(row_count, head_count, VDIM))


def shards(
    queries,
    kv_latent,
    rope_key,
    latent_gain,
    key_up,
    value_up,
    query_gain,
    key_gain,
    out_gain,
    out_proj,
    moe_input,
    moe_gain,
    expert_ids,
    route_weights,
    w_gate,
    w_up,
    w_down,
):
    tok_rows = queries.shape[0]
    head_count = key_up.shape[1] // NOPE
    query_pos = lax.axis_index("ep") * tok_rows + jnp.arange(tok_rows, dtype=jnp.int32)
    query_rot = make_queries(queries, query_gain, query_pos)
    inv_scale = QKD ** (-0.5)
    blocks_in = (
        lax.all_gather(kv_latent, "ep", axis=0, tiled=True),
        lax.all_gather(rope_key, "ep", axis=0, tiled=True),
    )
    key_pos = jnp.arange(blocks_in[0].shape[0], dtype=jnp.int32)
    key_rot, value_rows = make_keys(
        blocks_in[0], blocks_in[1], latent_gain, key_up, value_up, key_gain, key_pos
    )
    top_prev = jnp.full((head_count, tok_rows), -1e30, jnp.float32)
    key_pos = jnp.arange(key_rot.shape[0], dtype=jnp.int32)
    scores = (
        jnp.einsum("qhd,khd->hqk", query_rot, key_rot, preferred_element_type=jnp.float32)
        * inv_scale
    )
    visible = key_pos[None, :] <= query_pos[:, None]
    scores = jnp.where(visible[None], scores, -1e30)
    top_new = jnp.maximum(top_prev, jnp.max(scores, axis=-1))
    expo = jnp.exp(scores - top_new[..., None])
    total_new = jnp.sum(expo, axis=-1)
    accum_new = jnp.einsum(
        "hqk,khd->hqd", expo.astype(jnp.bfloat16), value_rows, preferred_element_type=jnp.float32
    )
    attn = (accum_new / total_new[..., None]).astype(jnp.bfloat16)
    attn = attn.transpose(1, 0, 2).reshape(tok_rows, head_count * VDIM)
    block_f = lax.all_gather(attn, "tp", axis=1, tiled=True).astype(jnp.float32)
    scaled = (block_f * out_gain[None, :]).astype(jnp.bfloat16)
    product = jnp.dot(scaled, out_proj, preferred_element_type=jnp.float32)
    product, squares = (product, jnp.sum(block_f * block_f, axis=-1))
    mixed = (product * lax.rsqrt(squares / out_gain.shape[0] + EPS)[:, None]).astype(jnp.bfloat16)
    row_count = moe_input.shape[0]
    top_count = expert_ids.shape[1]
    local_experts = w_gate.shape[0]
    ep_count = lax.axis_size("ep")
    expert_count = local_experts * ep_count
    stream_f = moe_input.astype(jnp.float32)
    normed = (
        stream_f * lax.rsqrt(jnp.mean(stream_f * stream_f, axis=-1, keepdims=True) + EPS) * moe_gain
    ).astype(jnp.bfloat16)
    flat_ids = expert_ids.reshape(-1)
    onehot = (flat_ids[:, None] == jnp.arange(expert_count, dtype=jnp.int32)[None, :]).astype(
        jnp.int32
    )
    slot_rank = jnp.sum((jnp.cumsum(onehot, axis=0) - onehot) * onehot, axis=1)
    slot_index = flat_ids * CAP + slot_rank
    token_index = jnp.arange(row_count * top_count, dtype=jnp.int32) // top_count
    slot_token = jnp.zeros((expert_count * CAP,), jnp.int32).at[slot_index].set(token_index)
    slot_used = jnp.zeros((expert_count * CAP,), jnp.bool_).at[slot_index].set(True)
    outgoing = jnp.where(slot_used[:, None], normed[slot_token], jnp.zeros((), jnp.bfloat16))
    outgoing = outgoing.reshape(ep_count, local_experts, CAP, normed.shape[1])
    piece_width = normed.shape[1] // lax.axis_size("tp")
    my_columns = lax.dynamic_slice_in_dim(
        outgoing, lax.axis_index("tp") * piece_width, piece_width, 3
    )
    arrived_part = lax.all_to_all(my_columns, "ep", split_axis=0, concat_axis=0, tiled=True)
    piece = lax.all_gather(arrived_part, "tp", axis=3, tiled=True)
    gate_acc = jnp.einsum("secd,edf->secf", piece, w_gate, preferred_element_type=jnp.float32)
    upper_acc = jnp.einsum("secd,edf->secf", piece, w_up, preferred_element_type=jnp.float32)
    hidden = (jax.nn.silu(gate_acc) * upper_acc).astype(jnp.bfloat16)
    out_cols = w_down.shape[2] // lax.axis_size("tp")
    term = jnp.einsum("secf,efd->dsec", hidden, w_down, preferred_element_type=jnp.float32)
    summed = lax.psum_scatter(
        term.reshape(lax.axis_size("tp") * out_cols, -1).astype(jnp.bfloat16),
        "tp",
        scatter_dimension=0,
        tiled=True,
    )
    expert_y = summed.T.reshape(ep_count, local_experts * CAP, out_cols)
    returned_rows = lax.all_to_all(expert_y, "ep", split_axis=0, concat_axis=0, tiled=True).reshape(
        expert_count * CAP, out_cols
    )
    picked = returned_rows[slot_index].reshape(row_count, top_count, out_cols).astype(jnp.float32)
    expert_out = jnp.sum(picked * route_weights[..., None], axis=1).astype(jnp.bfloat16)
    return (mixed, expert_out)


MESH = pl.DeviceIdType.MESH
GROUP = 8
PAD = 128


def group_cap():
    return GROUP * CAP // 2


def rdma(src, dst, send_sem, recv_sem, device):
    copy = pltpu.make_async_remote_copy(
        src_ref=src,
        dst_ref=dst,
        send_sem=send_sem,
        recv_sem=recv_sem,
        device_id=device,
        device_id_type=MESH,
    )
    copy.start()
    return copy


def arrived(dst, sem, device):
    pltpu.make_async_remote_copy(
        src_ref=dst,
        dst_ref=dst,
        send_sem=sem,
        recv_sem=sem,
        device_id=device,
        device_id_type=MESH,
    ).wait_recv()


def places(planes):
    ep = lax.axis_index("ep")
    tp = lax.axis_index("tp")
    plane = ep // 2
    core = ep % 2

    def along(offset):
        return (lax.rem(plane + offset + planes, planes) * 2 + core, tp)

    partner = (plane * 2 + 1 - core, tp)
    near_x = (ep, tp ^ 1)
    near_y = (ep, tp ^ 2)
    corner = (ep, tp ^ 3)
    return tp, along, partner, near_x, near_y, corner


def greet(peers):
    barrier = pltpu.get_barrier_semaphore()
    for peer in peers:
        pl.semaphore_signal(barrier, inc=1, device_id=peer, device_id_type=MESH)
    pl.semaphore_wait(barrier, len(peers))


def rope_table(total):
    half = ROPE // 2
    inverse = np.float32(THETA) ** (-np.arange(half, dtype=np.float32) / np.float32(half))
    angles = np.arange(total, dtype=np.float32)[None, :] * inverse[:, None]
    return np.concatenate([np.cos(angles), np.sin(angles)], axis=0).astype(np.float32)


def turn(first_half, second_half, cosine, sine):
    return (
        first_half * cosine - second_half * sine,
        second_half * cosine + first_half * sine,
    )


def to_column(row):
    size = row.shape[1]
    rows = lax.broadcasted_iota(jnp.int32, (size, size), 0)
    cols = lax.broadcasted_iota(jnp.int32, (size, size), 1)
    return jnp.sum(jnp.where(rows == cols, row, 0.0), axis=1, keepdims=True)


def layer_kernel(
    planes,
    queries_in,
    latent_in,
    rope_in,
    latent_gain_in,
    key_up_in,
    value_up_in,
    query_gain_in,
    key_gain_in,
    out_gain_in,
    out_proj_in,
    stream_in,
    moe_gain_in,
    ids_in,
    weights_in,
    gate_ref,
    up_ref,
    down_ref,
    table_in,
    mixed_ref,
    expert_ref,
    queries_v,
    latent_v,
    latent_gain_v,
    key_up_v,
    value_up_v,
    query_gain_v,
    key_gain_v,
    out_gain_v,
    out_proj_v,
    stream_v,
    moe_gain_v,
    ids_v,
    weights_v,
    table_v,
    wbuf,
    latents,
    ropes,
    outgoing,
    metas_out,
    rows_ref,
    metas,
    turned_q,
    turned_k,
    values_v,
    heads,
    select_t,
    place_v,
    place_t,
    slot_w,
    taken,
    gate_acc,
    up_acc,
    hidden_v,
    given,
    part,
    other,
    bx1,
    by1,
    bx2,
    by2,
    done,
    back,
    loc,
    ws,
    zs,
    zr,
    xs,
    xr,
    ks,
    kr,
    ps,
    pr,
    hs,
    hr,
    cs,
    cr,
    rs,
    rr,
    bs,
    br,
):
    f32, bf = jnp.float32, jnp.bfloat16
    ep = lax.axis_index("ep")
    plane, core = ep // 2, ep % 2
    tp, along, partner, near_x, near_y, corner = places(planes)
    peers = [along(d) for d in range(1, planes)] + [partner, near_x, near_y, corner]
    barrier = pltpu.get_barrier_semaphore()
    for peer in peers:
        pl.semaphore_signal(barrier, inc=1, device_id=peer, device_id_type=MESH)

    blocks = 2 * planes
    tokens, model = stream_in.shape
    cap, width = outgoing.shape[1], outgoing.shape[2]
    experts, hidden = gate_ref.shape[0], gate_ref.shape[2]
    row_total, slots = blocks * cap, blocks * CAP
    slot_total = experts * slots
    quarter_rows = tokens // 4
    half_r, half_w = quarter_rows // 2, width // 2
    low, high = pl.ds(0, half_w), pl.ds(half_w, half_w)
    halves = (low, high)
    head_count = key_up_in.shape[1] // NOPE
    order = list(range(1, planes))
    turned = (((0,), (0,)), ((), ()))
    across = (((1,), (1,)), ((), ()))

    loads = {}

    def load(name, source, target):
        copy = pltpu.make_async_copy(source, target, loc.at[len(loads)])
        copy.start()
        loads[name] = copy

    load("latent", latent_in, latent_v)
    load("latent_gain", latent_gain_in, latent_gain_v)
    load("rope", rope_in, ropes.at[0, 0])
    load("stream", stream_in, stream_v)
    load("moe_gain", moe_gain_in, moe_gain_v)
    load("ids", ids_in, ids_v)
    load("weights", weights_in, weights_v)

    sent = []

    def send(src, dst, send_sem, recv_sem, device):
        sent.append(rdma(src, dst, send_sem, recv_sem, device))

    def quarter(which):
        return pl.ds(pl.multiple_of(which * quarter_rows, quarter_rows), quarter_rows)

    loads["latent"].wait()
    loads["latent_gain"].wait()
    latent_f = latent_v[...].astype(f32)
    latents[0, 0] = (
        latent_f
        * lax.rsqrt(jnp.mean(latent_f * latent_f, axis=-1, keepdims=True) + EPS)
        * latent_gain_v[...]
    ).astype(bf)
    loads["rope"].wait()
    pl.semaphore_wait(barrier, len(peers))
    own_part = latents.at[0, 0, quarter(tp)]
    for d in order:
        send(own_part, latents.at[0, d, quarter(tp)], zs.at[0, d], zr.at[0, d], along(d))
        send(ropes.at[0, 0], ropes.at[0, d], zs.at[1, d], zr.at[1, d], along(d))
    send(latents.at[0, 0], latents.at[1, 0], ks.at[0, 0], kr.at[0, 0], partner)
    send(ropes.at[0, 0], ropes.at[1, 0], ks.at[1, 0], kr.at[1, 0], partner)

    loads["stream"].wait()
    loads["moe_gain"].wait()
    loads["ids"].wait()
    loads["weights"].wait()
    load("queries", queries_in, queries_v)
    load("query_gain", query_gain_in, query_gain_v)
    load("key_gain", key_gain_in, key_gain_v)
    load("table", table_in, table_v)
    load("key_up", key_up_in, key_up_v)
    load("value_up", value_up_in, value_up_v)
    gate_in, up_in, down_in = [], [], {}
    for s in range(4):
        depth = pl.ds(pl.multiple_of((tp ^ s) * width, width), width)
        gate_in.append(
            pltpu.make_async_copy(gate_ref.at[:, depth, :], wbuf.at[s], ws.at[0, s])
        )
        up_in.append(pltpu.make_async_copy(up_ref.at[:, depth, :], wbuf.at[4 + s], ws.at[1, s]))
        gate_in[s].start()
        up_in[s].start()
    down_slot = (1, 4, 0, 8)
    pieces = width // hidden

    def fetch_down(s):
        for piece in range(pieces):
            start = pl.multiple_of((tp ^ s) * width + piece * hidden, hidden)
            copy = pltpu.make_async_copy(
                down_ref.at[:, :, pl.ds(start, hidden)],
                wbuf.at[down_slot[s], :, pl.ds(piece * hidden, hidden), :],
                ws.at[2 + piece, s],
            )
            copy.start()
            down_in[s, piece] = copy

    fetch_down(3)
    load("out_gain", out_gain_in, out_gain_v)
    load("out_proj", out_proj_in, out_proj_v)

    ids = ids_v[...]
    local_ids = ids & (GROUP - 1)
    group = jnp.right_shift(ids[0:1], GROUP.bit_length() - 1)
    offset = jnp.where(group >= plane, group - plane, group - plane + planes)
    in_group = lax.broadcasted_iota(jnp.int32, (8, tokens), 0) == offset
    names = lax.broadcasted_iota(jnp.int32, (planes * GROUP, tokens), 0)
    hit = [names == offset * GROUP + local_ids[k : k + 1] for k in range(2)]
    counted = jnp.concatenate(
        [in_group.astype(f32), hit[0].astype(f32) + hit[1].astype(f32)], axis=0
    ).astype(bf)
    before = (
        lax.broadcasted_iota(jnp.int32, (tokens, tokens), 0)
        < lax.broadcasted_iota(jnp.int32, (tokens, tokens), 1)
    ).astype(f32).astype(bf)
    earlier = jnp.dot(counted, before, preferred_element_type=f32)
    rank = jnp.sum(jnp.where(in_group, earlier[0:8], 0.0), axis=0, keepdims=True).astype(jnp.int32)
    codes = [
        local_ids[k : k + 1].astype(f32) * CAP
        + jnp.sum(jnp.where(hit[k], earlier[8:], 0.0), axis=0, keepdims=True)
        + 1.0
        for k in range(2)
    ]
    route = weights_v[...]
    route_high = route.astype(bf).astype(f32)
    route_low = route - route_high
    line = lax.broadcasted_iota(jnp.int32, (16, tokens), 0)
    meta = jnp.zeros((16, tokens), f32)
    meta_rows = codes + [route_high[0:1], route_high[1:2], route_low[0:1], route_low[1:2]]
    for i, row in enumerate(meta_rows):
        meta = jnp.where(line == i, row, meta)
    select = (
        lax.broadcasted_iota(jnp.int32, (planes * cap, tokens), 0) == offset * cap + rank
    ).astype(f32)
    select_b = select.astype(bf)
    wide = (
        lax.broadcasted_iota(jnp.int32, (planes * PAD, tokens), 0) == offset * PAD + rank
    ).astype(f32).astype(bf)
    meta_all = lax.dot_general(meta.astype(bf), wide, across, preferred_element_type=f32).astype(bf)
    for d in range(planes):
        metas_out[d] = meta_all[:, d * PAD : (d + 1) * PAD]
    metas[0, 0] = meta_all[:, 0:PAD]

    stream_f = stream_v[...].astype(f32)
    scale = lax.rsqrt(jnp.mean(stream_f * stream_f, axis=-1, keepdims=True) + EPS)
    own_cols = pl.ds(pl.multiple_of(tp * width, width), width)
    own_normed = (
        stream_v[:, own_cols].astype(f32) * scale * moe_gain_v[:, own_cols]
    ).astype(bf)
    out_rows = jnp.dot(select_b[cap:], own_normed, preferred_element_type=f32).astype(bf)
    for d in order:
        outgoing[d] = out_rows[(d - 1) * cap : d * cap]
    for d in order:
        send(outgoing.at[d], rows_ref.at[tp, 0, d], zs.at[3, d], zr.at[3, d], along(d))
        send(metas_out.at[d], metas.at[0, d], zs.at[2, d], zr.at[2, d], along(d))
    for q in range(4):
        cols = slice(q * width, (q + 1) * width)
        normed_q = (stream_v[:, cols].astype(f32) * scale * moe_gain_v[:, cols]).astype(bf)
        rows_ref[q, 0, 0] = jnp.dot(select_b[0:cap], normed_q, preferred_element_type=f32).astype(bf)
    send(rows_ref.at[:, 0, 0], rows_ref.at[:, 1, 0], ps.at[0, 0], pr.at[0, 0], partner)
    send(metas_out.at[0], metas.at[1, 0], ks.at[2, 0], kr.at[2, 0], partner)
    select_t[...] = jnp.transpose(select).astype(bf)

    def first(kind, d):
        if kind == 0:
            mine = latents.at[0, d, quarter(tp)]
            arrived(mine, zr.at[0, d], along(-d))
        else:
            mine = rows_ref.at[tp, 0, d]
            arrived(mine, zr.at[3, d], along(-d))
        send(mine, mine, xs.at[kind, 0, d], xr.at[kind, 0, d], near_x)
        send(mine, mine, xs.at[kind, 1, d], xr.at[kind, 1, d], near_y)
        if kind == 0:
            arrived(ropes.at[0, d], zr.at[1, d], along(-d))
            send(ropes.at[0, d], ropes.at[1, d], ks.at[1, d], kr.at[1, d], partner)
        else:
            send(mine, rows_ref.at[tp, 1, d], ps.at[0, d], pr.at[0, d], partner)
            arrived(metas.at[0, d], zr.at[2, d], along(-d))
            send(metas.at[0, d], metas.at[1, d], ks.at[2, d], kr.at[2, d], partner)

    def half_of(kind, flip, d, side):
        if kind == 0:
            start = (tp ^ flip) * quarter_rows + side * half_r
            return latents.at[0, d, pl.ds(pl.multiple_of(start, half_r), half_r)]
        return rows_ref.at[tp ^ flip, 0, d, :, halves[side]]

    def whole_of(kind, flip, d):
        if kind == 0:
            return latents.at[0, d, quarter(tp ^ flip)]
        return rows_ref.at[tp ^ flip, 0, d]

    def second(kind, d):
        arrived(whole_of(kind, 1, d), xr.at[kind, 0, d], near_x)
        piece = half_of(kind, 1, d, 0)
        send(piece, piece, xs.at[kind, 2, d], xr.at[kind, 2, d], near_y)
        arrived(whole_of(kind, 2, d), xr.at[kind, 1, d], near_y)
        piece = half_of(kind, 2, d, 1)
        send(piece, piece, xs.at[kind, 3, d], xr.at[kind, 3, d], near_x)
        if kind == 1:
            for flip in (1, 2):
                send(
                    rows_ref.at[tp ^ flip, 0, d],
                    rows_ref.at[tp ^ flip, 1, d],
                    ps.at[flip, d],
                    pr.at[flip, d],
                    partner,
                )

    def third(kind, d):
        arrived(half_of(kind, 3, d, 0), xr.at[kind, 2, d], near_y)
        arrived(half_of(kind, 3, d, 1), xr.at[kind, 3, d], near_x)
        if kind == 0:
            send(latents.at[0, d], latents.at[1, d], ks.at[0, d], kr.at[0, d], partner)
        else:
            mine = rows_ref.at[tp ^ 3, 0, d]
            send(mine, rows_ref.at[tp ^ 3, 1, d], ps.at[3, d], pr.at[3, d], partner)

    def run_steps(kind_steps):
        for stage, kind, d in kind_steps:
            (first, second, third)[stage - 1](kind, d)

    loads["queries"].wait()
    loads["query_gain"].wait()
    loads["key_gain"].wait()
    loads["table"].wait()
    half = ROPE // 2
    query_t = jnp.transpose(queries_v[...].astype(f32))
    gain_q = to_column(query_gain_v[...])
    gain_k = to_column(key_gain_v[...])
    own_lanes = pl.ds(pl.multiple_of(ep * tokens, tokens), tokens)
    cos_q, sin_q = table_v[0:half, own_lanes], table_v[half:ROPE, own_lanes]
    for h in range(head_count):
        z = query_t[h * QKD : (h + 1) * QKD]
        z = z * lax.rsqrt(jnp.mean(z * z, axis=0, keepdims=True) + EPS) * gain_q
        turned_a, turned_b = turn(z[NOPE : NOPE + half], z[NOPE + half :], cos_q, sin_q)
        turned_q[h] = jnp.concatenate([z[:NOPE], turned_a, turned_b], axis=0).astype(bf)

    run_steps([(1, 0, 1), (1, 0, 2), (2, 0, 1), (1, 0, 3), (2, 0, 2), (3, 0, 1)])
    run_steps([(1, 1, 1), (2, 0, 3), (3, 0, 2), (3, 0, 3)])

    for d in range(planes):
        arrived(latents.at[1, d], kr.at[0, d], partner)
        arrived(ropes.at[1, d], kr.at[1, d], partner)
    loads["key_up"].wait()
    loads["value_up"].wait()
    starts = [
        ((plane - d + planes) % planes * 2 + (core ^ parity)) * tokens
        for parity in range(2)
        for d in range(planes)
    ]
    key_total = blocks * tokens
    key_rows = latents[...].reshape(key_total, latents.shape[-1])
    key_t = lax.dot_general(
        key_up_v[...], key_rows, (((0,), (1,)), ((), ())), preferred_element_type=f32
    )
    key_t = key_t.astype(bf).astype(f32)
    values_v[...] = jnp.dot(key_rows, value_up_v[...], preferred_element_type=f32).astype(bf)
    run_steps([(1, 1, 2), (2, 1, 1)])
    rope_t = jnp.concatenate(
        [ropes[parity, d].astype(f32) for parity in range(2) for d in range(planes)], axis=1
    )
    lanes = [pl.ds(pl.multiple_of(start, tokens), tokens) for start in starts]
    cos_k = jnp.concatenate([table_v[0:half, lane] for lane in lanes], axis=1)
    sin_k = jnp.concatenate([table_v[half:ROPE, lane] for lane in lanes], axis=1)
    lane_ids = lax.broadcasted_iota(jnp.int32, (1, tokens), 1)
    key_pos = jnp.concatenate([lane_ids + start for start in starts], axis=1)
    query_pos = ep * tokens + lax.broadcasted_iota(jnp.int32, (tokens, 1), 0)
    visible = key_pos <= query_pos
    rope_squares = jnp.sum(rope_t * rope_t, axis=0, keepdims=True)
    for h in range(head_count):
        nope = key_t[h * NOPE : (h + 1) * NOPE]
        squares = jnp.sum(nope * nope, axis=0, keepdims=True) + rope_squares
        factor = lax.rsqrt(squares / QKD + EPS)
        nope = nope * factor * gain_k[:NOPE]
        spun = rope_t * factor * gain_k[NOPE:]
        turned_a, turned_b = turn(spun[:half], spun[half:], cos_k, sin_k)
        turned_k[h] = jnp.concatenate([nope, turned_a, turned_b], axis=0).astype(bf)
    head_of = jnp.right_shift(
        lax.broadcasted_iota(jnp.int32, (tokens, head_count * VDIM), 1), VDIM.bit_length() - 1
    )

    def attend(h, attn):
        scores = (
            lax.dot_general(turned_q[h], turned_k[h], turned, preferred_element_type=f32)
            * QKD ** (-0.5)
        )
        scores = jnp.where(visible, scores, -1e30)
        expo = jnp.exp(scores - jnp.max(scores, axis=-1, keepdims=True))
        total = jnp.sum(expo, axis=-1, keepdims=True)
        mixed_h = jnp.dot(expo.astype(bf), values_v[...], preferred_element_type=f32) / total
        return jnp.where(head_of == h, mixed_h, attn)

    attn = jnp.zeros((tokens, head_count * VDIM), f32)
    for h in range(head_count // 2):
        attn = attend(h, attn)
    run_steps([(1, 1, 3)])
    for h in range(head_count // 2, head_count):
        attn = attend(h, attn)
    heads[tp] = attn.astype(bf)
    run_steps([(2, 1, 2), (3, 1, 1)])

    for d in range(planes):
        arrived(metas.at[1, d], kr.at[2, d], partner)
    spot = (
        lax.broadcasted_iota(jnp.int32, (cap, PAD), 0)
        == lax.broadcasted_iota(jnp.int32, (cap, PAD), 1)
    ).astype(f32).astype(bf)
    info = jnp.concatenate(
        [
            lax.dot_general(spot, metas[parity, d], across, preferred_element_type=f32)
            for parity in range(2)
            for d in range(planes)
        ],
        axis=0,
    )
    info_b = info.astype(bf)
    block_of = jnp.concatenate(
        [jnp.full((cap, 1), block, jnp.int32) for block in range(blocks)], axis=0
    )
    slot_ids = lax.broadcasted_iota(jnp.int32, (row_total, slot_total), 1)
    place = jnp.zeros((row_total, slot_total), f32)
    placed_t = jnp.zeros((slot_total, row_total), f32)
    slot_weights = jnp.zeros((slot_total, 1), f32)
    for k in range(2):
        column = info[:, k : k + 1]
        code = column.astype(jnp.int32) - 1 - core * (experts * CAP)
        inside = (column > 0.5) & (code >= 0) & (code < experts * CAP)
        expert = jnp.zeros_like(code)
        for e in range(1, experts):
            expert += (code >= e * CAP).astype(jnp.int32)
        where = expert * (slots - CAP) + block_of * CAP + code
        match = (slot_ids == jnp.where(inside, where, -1)).astype(f32)
        match_t = jnp.transpose(match)
        place += match
        placed_t += match_t
        found = jnp.dot(match_t.astype(bf), info_b, preferred_element_type=f32)
        slot_weights += found[:, 2 + k : 3 + k] + found[:, 4 + k : 5 + k]
    place_v[...] = place.astype(bf)
    place_t[...] = placed_t.astype(bf)
    slot_w[...] = slot_weights
    run_steps([(2, 1, 3), (3, 1, 2)])
    for i, peer in enumerate((near_x, near_y, corner)):
        send(heads.at[tp], heads.at[tp], hs.at[i], hr.at[i], peer)

    def feed(s):
        for d in range(planes):
            if s == 0 and d == 0:
                arrived(rows_ref.at[:, 1, 0], pr.at[0, 0], partner)
            elif d > 0:
                arrived(rows_ref.at[tp ^ s, 1, d], pr.at[s, d], partner)
        rows = rows_ref[tp ^ s].reshape(row_total, width)
        taken[...] = jnp.dot(place_t[...], rows, preferred_element_type=f32).astype(bf)
        gate_in[s].wait()
        up_in[s].wait()
        for e in range(experts):
            mine = slice(e * slots, (e + 1) * slots)
            picked = taken[mine, :]
            gate = jnp.dot(picked, wbuf[s, e], preferred_element_type=f32)
            upper = jnp.dot(picked, wbuf[4 + s, e], preferred_element_type=f32)
            if s > 0:
                gate += gate_acc[e]
                upper += up_acc[e]
            if s < 3:
                gate_acc[e] = gate
                up_acc[e] = upper
            else:
                hidden_v[mine, :] = (
                    gate / (1.0 + jnp.exp(-gate)) * upper * slot_w[mine, :]
                ).astype(bf)

    feed(0)
    fetch_down(2)
    fetch_down(1)
    run_steps([(3, 1, 3)])
    feed(1)
    fetch_down(0)
    feed(2)
    feed(3)

    def spread(s):
        for piece in range(pieces):
            down_in[s, piece].wait()
        for e in range(experts):
            mine = slice(e * slots, (e + 1) * slots)
            for piece in range(pieces):
                cols = slice(piece * hidden, (piece + 1) * hidden)
                given[mine, cols] = jnp.dot(
                    hidden_v[mine, :], wbuf[down_slot[s], e, cols, :], preferred_element_type=f32
                ).astype(bf)
        summed = jnp.dot(place_v[...], given[...], preferred_element_type=f32).astype(bf)
        part[s] = summed.reshape(2, planes, cap, width)
        for d in range(planes):
            send(part.at[s, 1, d], other.at[s, d], cs.at[s, d], cr.at[s, d], partner)

    def join(s):
        for d in range(planes):
            arrived(other.at[s, d], cr.at[s, d], partner)
            part[s, 0, d] = (part[s, 0, d].astype(f32) + other[s, d].astype(f32)).astype(bf)

    away = order + [0]

    def start_rest(d):
        send(part.at[2, 0, d, :, high], by2.at[d, :, high], rs.at[2, d], rr.at[2, d], near_y)
        send(part.at[1, 0, d, :, low], bx2.at[d, :, low], rs.at[3, d], rr.at[3, d], near_x)

    def pass_on(d):
        arrived(bx1.at[d], rr.at[0, d], near_x)
        part[2, 0, d, :, low] = (
            part[2, 0, d, :, low].astype(f32) + bx1[d].astype(f32)
        ).astype(bf)
        send(part.at[2, 0, d, :, low], by2.at[d, :, low], rs.at[4, d], rr.at[4, d], near_y)
        arrived(by1.at[d], rr.at[1, d], near_y)
        part[1, 0, d, :, high] = (
            part[1, 0, d, :, high].astype(f32) + by1[d].astype(f32)
        ).astype(bf)
        send(part.at[1, 0, d, :, high], bx2.at[d, :, high], rs.at[5, d], rr.at[5, d], near_x)

    def finish(d):
        arrived(by2.at[d, :, high], rr.at[2, d], near_y)
        arrived(bx2.at[d, :, low], rr.at[3, d], near_x)
        arrived(by2.at[d, :, low], rr.at[4, d], near_y)
        arrived(bx2.at[d, :, high], rr.at[5, d], near_x)
        full = (
            part[0, 0, d].astype(f32) + bx2[d].astype(f32) + by2[d].astype(f32)
        ).astype(bf)
        if d == 0:
            back[0] = full
        else:
            done[d] = full
            send(done.at[d], back.at[d], bs.at[d], br.at[d], along(-d))

    spread(3)
    spread(2)
    join(3)
    for d in away:
        send(part.at[3, 0, d, :, low], bx1.at[d], rs.at[0, d], rr.at[0, d], near_x)
        send(part.at[3, 0, d, :, high], by1.at[d], rs.at[1, d], rr.at[1, d], near_y)
    spread(1)
    join(2)
    join(1)
    for d in order:
        start_rest(d)
    spread(0)
    for d in order:
        pass_on(d)
    start_rest(0)
    pass_on(0)
    join(0)

    for i, peer in enumerate((near_x, near_y, corner)):
        arrived(heads.at[tp ^ (i + 1)], hr.at[i], peer)
    loads["out_gain"].wait()
    loads["out_proj"].wait()
    block_f = jnp.concatenate([heads[q] for q in range(4)], axis=1).astype(f32)
    squares = jnp.mean(block_f * block_f, axis=-1, keepdims=True)
    scaled = (block_f * out_gain_v[...]).astype(bf)
    product = jnp.dot(scaled, out_proj_v[...], preferred_element_type=f32)
    mixed_ref[...] = (product * lax.rsqrt(squares + EPS)).astype(bf)

    for d in away:
        finish(d)
    for d in order:
        arrived(back.at[d], br.at[d], along(d))
    expert_ref[...] = jnp.dot(
        select_t[...], back[...].reshape(planes * cap, width), preferred_element_type=f32
    ).astype(bf)
    for copy in sent:
        copy.wait_send()


def fused(
    queries,
    kv_latent,
    rope_key,
    latent_gain,
    key_up,
    value_up,
    query_gain,
    key_gain,
    out_gain,
    out_proj,
    moe_input,
    moe_gain,
    expert_ids,
    route_weights,
    w_gate,
    w_up,
    w_down,
):
    f32, bf, i32 = jnp.float32, jnp.bfloat16, jnp.int32
    planes = lax.axis_size("ep") // 2
    tokens, model = moe_input.shape
    width = model // lax.axis_size("tp")
    experts, _, hidden = w_gate.shape
    cap = group_cap()
    blocks = 2 * planes
    row_total, slots = blocks * cap, blocks * CAP
    slot_total = experts * slots
    rank = kv_latent.shape[1]
    head_count = key_up.shape[1] // NOPE
    total = tokens * lax.axis_size("ep")
    v_cols = value_up.shape[1]
    table = jnp.asarray(rope_table(total))
    dma = pltpu.SemaphoreType.DMA
    vmem = pltpu.VMEM
    operands = (
        queries,
        kv_latent,
        rope_key.T,
        latent_gain.reshape(1, -1),
        key_up,
        value_up,
        query_gain.reshape(1, -1),
        key_gain.reshape(1, -1),
        out_gain.reshape(1, -1),
        out_proj,
        moe_input,
        moe_gain.reshape(1, -1),
        expert_ids.T,
        route_weights.T,
        w_gate,
        w_up,
        w_down,
        table,
    )
    mixed, expert_out = pl.pallas_call(
        functools.partial(layer_kernel, planes),
        out_shape=(
            jax.ShapeDtypeStruct((tokens, out_proj.shape[1]), bf),
            jax.ShapeDtypeStruct((tokens, width), bf),
        ),
        in_specs=[pl.BlockSpec(memory_space=pl.ANY)] * len(operands),
        out_specs=(pl.BlockSpec(memory_space=pltpu.VMEM),) * 2,
        scratch_shapes=[
            vmem(queries.shape, bf),
            vmem(kv_latent.shape, bf),
            vmem((1, rank), f32),
            vmem(key_up.shape, bf),
            vmem(value_up.shape, bf),
            vmem((1, QKD), f32),
            vmem((1, QKD), f32),
            vmem((1, out_gain.shape[0]), f32),
            vmem(out_proj.shape, bf),
            vmem(moe_input.shape, bf),
            vmem((1, model), f32),
            vmem((2, tokens), i32),
            vmem((2, tokens), f32),
            vmem(table.shape, f32),
            vmem((9, experts, width, hidden), bf),
            vmem((2, planes, tokens, rank), bf),
            vmem((2, planes, ROPE, tokens), bf),
            vmem((planes, cap, width), bf),
            vmem((planes, 16, PAD), bf),
            vmem((4, 2, planes, cap, width), bf),
            vmem((2, planes, 16, PAD), bf),
            vmem((head_count, QKD, tokens), bf),
            vmem((head_count, QKD, total), bf),
            vmem((total, v_cols), bf),
            vmem((4, tokens, v_cols), bf),
            vmem((tokens, planes * cap), bf),
            vmem((row_total, slot_total), bf),
            vmem((slot_total, row_total), bf),
            vmem((slot_total, 1), f32),
            vmem((slot_total, width), bf),
            vmem((experts, slots, hidden), f32),
            vmem((experts, slots, hidden), f32),
            vmem((slot_total, hidden), bf),
            vmem((slot_total, width), bf),
            vmem((4, 2, planes, cap, width), bf),
            vmem((4, planes, cap, width), bf),
            vmem((planes, cap, width // 2), bf),
            vmem((planes, cap, width // 2), bf),
            vmem((planes, cap, width), bf),
            vmem((planes, cap, width), bf),
            vmem((planes, cap, width), bf),
            vmem((planes, cap, width), bf),
            dma((15,)),
            dma((4, 4)),
            dma((4, planes)),
            dma((4, planes)),
            dma((2, 4, planes)),
            dma((2, 4, planes)),
            dma((3, planes)),
            dma((3, planes)),
            dma((4, planes)),
            dma((4, planes)),
            dma((3,)),
            dma((3,)),
            dma((4, planes)),
            dma((4, planes)),
            dma((6, planes)),
            dma((6, planes)),
            dma((planes,)),
            dma((planes,)),
        ],
        compiler_params=pltpu.CompilerParams(
            collective_id=0, has_side_effects=True, vmem_limit_bytes=67043328
        ),
        name="layer",
    )(*operands)
    return (mixed, expert_out)


def layer(*arrays):
    gate, stream = arrays[14], arrays[10]
    tp_count, ep_count = lax.axis_size("tp"), lax.axis_size("ep")
    fits = (
        tp_count == 4
        and ep_count % 2 == 0
        and ep_count // 2 <= GROUP
        and 2 * gate.shape[0] == GROUP
        and stream.shape[0] == PAD
        and stream.shape[1] // tp_count == 2 * gate.shape[2]
    )
    return fused(*arrays) if fits else shards(*arrays)


def solution(mesh):
    in_specs = (
        P("ep", "tp"),
        P("ep", None),
        P("ep", None),
        P(),
        P(None, "tp"),
        P(None, "tp"),
        P(),
        P(),
        P(),
        P(None, "tp"),
        P("ep", None),
        P(),
        P("ep", None),
        P("ep", None),
        P("ep", None, "tp"),
        P("ep", None, "tp"),
        P("ep", "tp", None),
    )
    out_specs = (P("ep", "tp"), P("ep", "tp"))
    return jax.shard_map(layer, mesh=mesh, in_specs=in_specs, out_specs=out_specs, check_vma=False)
```

time: 100 us -> 72.1 us (0.72)
  matrix products: 9.99 us -> 0 us
  other arithmetic: 9.19 us -> 0 us
  Pallas kernels: 74.4 us -> 67.9 us
  local copies, waits for them, and re-layouts: 5.28 us -> 3.34 us
    dot_general x9 -> x0, matrix products: 9.99 us -> none  [the longest x1 2.77 us: make_keys(): jnp.dot(latent_n, value_up, preferred_element_type=jnp.float32)]
    pallas_call x2 -> x1, Pallas kernels: 74.4 us -> 67.9 us  [fused(): pl.pallas_call(functools.partial(layer_kernel, planes), out_shape=(jax.Sh...]
    reduce_sum x8 -> x0, other arithmetic: 4.11 us -> none  [the longest x1 1.6 us: make_keys(): jnp.mean(latent_f * latent_f, axis=-1, keepdims=True) + EPS]
    unnamed x34 -> x2, local copies, waits for them, and re-layouts: 3.72 us -> 3.34 us
where the time goes in v1:
time: 72.1 us; the launch traced here: 71.9 us
  Pallas kernels  67.9 us (94%)
  local copies, waits for them, and re-layouts  3.34 us (5%)
    pallas_call x1, Pallas kernels, fused(): pl.pallas_call(functools.partial(layer_kernel, planes), out_shape=(jax.Sh...  67.9 us
    unnamed x2, local copies, waits for them, and re-layouts  3.34 us

profile of v1, /device:TPU:0, one launch (start us, length us, event | category | flops | bytes accessed | tf_op | source)
XLA Modules:
  0.0 71.9 jit_solution(16700850022707100800)
XLA Ops:
  0.6 67.9 %layer.1 = (bf16[128,1024]{1,0:T(8,128)(2,1)}, bf16[128,1024]{1,0:T(8,128)(2,1)}) custom-call(bf16[128,384]{1,0:T(8,128)(2,1)} %queries_in.1, bf16[128,512]{1,0:T(8,128)(2,1)} %latent_in.1, bf16[32,128]{1,0:T(8,128)(2,1)} %bitcast.9, f32[1,512]{1,0:T(1,128)} %bitcast.11, bf16[512,256]{1,0:T(8,128)(2,1)} %key_up_in.1, bf16[512,256]{1,0:T(8,128)(2,1)} %value_up_in.1, ...), custom_call_target="tpu_custom_call" | custom-call | tf_op jit(solution)/shard_map/layer/pallas_call | solution.py:865
  68.6 1.7 %copy.22 = bf16[128,1024]{1,0:T(8,128)(2,1)} copy(bf16[128,1024]{1,0:T(8,128)(2,1)} %get-tuple-element.4) | data formatting | bytes 524288
  70.2 1.7 %copy.23 = bf16[128,1024]{1,0:T(8,128)(2,1)} copy(bf16[128,1024]{1,0:T(8,128)(2,1)} %get-tuple-element.5) | data formatting | bytes 524288

commit v2 on v1

--- a/solution.py
+++ b/solution.py
@@ -357,7 +357,8 @@
     low, high = pl.ds(0, half_w), pl.ds(half_w, half_w)
     halves = (low, high)
     head_count = key_up_in.shape[1] // NOPE
-    order = list(range(1, planes))
+    order = sorted(range(1, planes), key=lambda d: (min(d, planes - d), d))
+    away = sorted(range(1, planes), key=lambda d: (-min(d, planes - d), d)) + [0]
     turned = (((0,), (0,)), ((), ()))
     across = (((1,), (1,)), ((), ()))
 
@@ -368,76 +369,30 @@
         copy.start()
         loads[name] = copy
 
+    load("ids", ids_in, ids_v)
+    load("weights", weights_in, weights_v)
+    load("stream", stream_in, stream_v)
+    load("moe_gain", moe_gain_in, moe_gain_v)
     load("latent", latent_in, latent_v)
     load("latent_gain", latent_gain_in, latent_gain_v)
     load("rope", rope_in, ropes.at[0, 0])
-    load("stream", stream_in, stream_v)
-    load("moe_gain", moe_gain_in, moe_gain_v)
-    load("ids", ids_in, ids_v)
-    load("weights", weights_in, weights_v)
-
-    sent = []
-
-    def send(src, dst, send_sem, recv_sem, device):
-        sent.append(rdma(src, dst, send_sem, recv_sem, device))
-
-    def quarter(which):
-        return pl.ds(pl.multiple_of(which * quarter_rows, quarter_rows), quarter_rows)
-
-    loads["latent"].wait()
-    loads["latent_gain"].wait()
-    latent_f = latent_v[...].astype(f32)
-    latents[0, 0] = (
-        latent_f
-        * lax.rsqrt(jnp.mean(latent_f * latent_f, axis=-1, keepdims=True) + EPS)
-        * latent_gain_v[...]
-    ).astype(bf)
-    loads["rope"].wait()
-    pl.semaphore_wait(barrier, len(peers))
-    own_part = latents.at[0, 0, quarter(tp)]
-    for d in order:
-        send(own_part, latents.at[0, d, quarter(tp)], zs.at[0, d], zr.at[0, d], along(d))
-        send(ropes.at[0, 0], ropes.at[0, d], zs.at[1, d], zr.at[1, d], along(d))
-    send(latents.at[0, 0], latents.at[1, 0], ks.at[0, 0], kr.at[0, 0], partner)
-    send(ropes.at[0, 0], ropes.at[1, 0], ks.at[1, 0], kr.at[1, 0], partner)
-
-    loads["stream"].wait()
-    loads["moe_gain"].wait()
-    loads["ids"].wait()
-    loads["weights"].wait()
     load("queries", queries_in, queries_v)
     load("query_gain", query_gain_in, query_gain_v)
     load("key_gain", key_gain_in, key_gain_v)
     load("table", table_in, table_v)
     load("key_up", key_up_in, key_up_v)
     load("value_up", value_up_in, value_up_v)
-    gate_in, up_in, down_in = [], [], {}
-    for s in range(4):
-        depth = pl.ds(pl.multiple_of((tp ^ s) * width, width), width)
-        gate_in.append(
-            pltpu.make_async_copy(gate_ref.at[:, depth, :], wbuf.at[s], ws.at[0, s])
-        )
-        up_in.append(pltpu.make_async_copy(up_ref.at[:, depth, :], wbuf.at[4 + s], ws.at[1, s]))
-        gate_in[s].start()
-        up_in[s].start()
-    down_slot = (1, 4, 0, 8)
-    pieces = width // hidden
-
-    def fetch_down(s):
-        for piece in range(pieces):
-            start = pl.multiple_of((tp ^ s) * width + piece * hidden, hidden)
-            copy = pltpu.make_async_copy(
-                down_ref.at[:, :, pl.ds(start, hidden)],
-                wbuf.at[down_slot[s], :, pl.ds(piece * hidden, hidden), :],
-                ws.at[2 + piece, s],
-            )
-            copy.start()
-            down_in[s, piece] = copy
-
-    fetch_down(3)
-    load("out_gain", out_gain_in, out_gain_v)
-    load("out_proj", out_proj_in, out_proj_v)
-
+
+    sent = []
+
+    def send(src, dst, send_sem, recv_sem, device):
+        sent.append(rdma(src, dst, send_sem, recv_sem, device))
+
+    def quarter(which):
+        return pl.ds(pl.multiple_of(which * quarter_rows, quarter_rows), quarter_rows)
+
+    loads["ids"].wait()
+    loads["weights"].wait()
     ids = ids_v[...]
     local_ids = ids & (GROUP - 1)
     group = jnp.right_shift(ids[0:1], GROUP.bit_length() - 1)
@@ -480,6 +435,35 @@
         metas_out[d] = meta_all[:, d * PAD : (d + 1) * PAD]
     metas[0, 0] = meta_all[:, 0:PAD]
 
+    loads["stream"].wait()
+    loads["moe_gain"].wait()
+    gate_in, up_in, down_in = [], [], {}
+    for s in range(4):
+        depth = pl.ds(pl.multiple_of((tp ^ s) * width, width), width)
+        gate_in.append(
+            pltpu.make_async_copy(gate_ref.at[:, depth, :], wbuf.at[s], ws.at[0, s])
+        )
+        up_in.append(pltpu.make_async_copy(up_ref.at[:, depth, :], wbuf.at[4 + s], ws.at[1, s]))
+        gate_in[s].start()
+        up_in[s].start()
+    down_slot = (1, 4, 0, 8)
+    pieces = width // hidden
+
+    def fetch_down(s):
+        for piece in range(pieces):
+            start = pl.multiple_of((tp ^ s) * width + piece * hidden, hidden)
+            copy = pltpu.make_async_copy(
+                down_ref.at[:, :, pl.ds(start, hidden)],
+                wbuf.at[down_slot[s], :, pl.ds(piece * hidden, hidden), :],
+                ws.at[2 + piece, s],
+            )
+            copy.start()
+            down_in[s, piece] = copy
+
+    fetch_down(3)
+    load("out_gain", out_gain_in, out_gain_v)
+    load("out_proj", out_proj_in, out_proj_v)
+
     stream_f = stream_v[...].astype(f32)
     scale = lax.rsqrt(jnp.mean(stream_f * stream_f, axis=-1, keepdims=True) + EPS)
     own_cols = pl.ds(pl.multiple_of(tp * width, width), width)
@@ -489,6 +473,7 @@
     out_rows = jnp.dot(select_b[cap:], own_normed, preferred_element_type=f32).astype(bf)
     for d in order:
         outgoing[d] = out_rows[(d - 1) * cap : d * cap]
+    pl.semaphore_wait(barrier, len(peers))
     for d in order:
         send(outgoing.at[d], rows_ref.at[tp, 0, d], zs.at[3, d], zr.at[3, d], along(d))
         send(metas_out.at[d], metas.at[0, d], zs.at[2, d], zr.at[2, d], along(d))
@@ -498,6 +483,15 @@
         rows_ref[q, 0, 0] = jnp.dot(select_b[0:cap], normed_q, preferred_element_type=f32).astype(bf)
     send(rows_ref.at[:, 0, 0], rows_ref.at[:, 1, 0], ps.at[0, 0], pr.at[0, 0], partner)
     send(metas_out.at[0], metas.at[1, 0], ks.at[2, 0], kr.at[2, 0], partner)
+    loads["latent"].wait()
+    loads["latent_gain"].wait()
+    latent_f = latent_v[...].astype(f32)
+    latents[0, 0] = (
+        latent_f
+        * lax.rsqrt(jnp.mean(latent_f * latent_f, axis=-1, keepdims=True) + EPS)
+        * latent_gain_v[...]
+    ).astype(bf)
+    loads["rope"].wait()
     select_t[...] = jnp.transpose(select).astype(bf)
 
     def first(kind, d):
@@ -554,10 +548,6 @@
             mine = rows_ref.at[tp ^ 3, 0, d]
             send(mine, rows_ref.at[tp ^ 3, 1, d], ps.at[3, d], pr.at[3, d], partner)
 
-    def run_steps(kind_steps):
-        for stage, kind, d in kind_steps:
-            (first, second, third)[stage - 1](kind, d)
-
     loads["queries"].wait()
     loads["query_gain"].wait()
     loads["key_gain"].wait()
@@ -574,9 +564,200 @@
         turned_a, turned_b = turn(z[NOPE : NOPE + half], z[NOPE + half :], cos_q, sin_q)
         turned_q[h] = jnp.concatenate([z[:NOPE], turned_a, turned_b], axis=0).astype(bf)
 
-    run_steps([(1, 0, 1), (1, 0, 2), (2, 0, 1), (1, 0, 3), (2, 0, 2), (3, 0, 1)])
-    run_steps([(1, 1, 1), (2, 0, 3), (3, 0, 2), (3, 0, 3)])
-
+    each = planes * CAP
+
+    def both(ref, e):
+        mine = slice(e * each, (e + 1) * each)
+        return jnp.concatenate([ref[0, mine, :], ref[1, mine, :]], axis=0)
+
+    def feed(s):
+        for d in range(planes):
+            if s == 0 and d == 0:
+                arrived(rows_ref.at[:, 1, 0], pr.at[0, 0], partner)
+            elif d > 0:
+                arrived(rows_ref.at[tp ^ s, 1, d], pr.at[s, d], partner)
+        for parity in range(2):
+            rows = rows_ref[tp ^ s, parity].reshape(planes * cap, width)
+            taken[parity] = jnp.dot(
+                place_t[parity], rows, preferred_element_type=f32
+            ).astype(bf)
+        gate_in[s].wait()
+        up_in[s].wait()
+        for e in range(experts):
+            picked = both(taken, e)
+            gate = jnp.dot(picked, wbuf[s, e], preferred_element_type=f32)
+            upper = jnp.dot(picked, wbuf[4 + s, e], preferred_element_type=f32)
+            if s > 0:
+                gate += gate_acc[e]
+                upper += up_acc[e]
+            if s < 3:
+                gate_acc[e] = gate
+                up_acc[e] = upper
+            else:
+                act = (gate / (1.0 + jnp.exp(-gate)) * upper * both(slot_w, e)).astype(bf)
+                for parity in range(2):
+                    hidden_v[parity, e * each : (e + 1) * each] = act[
+                        parity * each : (parity + 1) * each
+                    ]
+
+    first(1, order[0])
+    first(1, order[1])
+    second(1, order[0])
+    first(1, order[2])
+    own_part = latents.at[0, 0, quarter(tp)]
+    for d in order:
+        send(own_part, latents.at[0, d, quarter(tp)], zs.at[0, d], zr.at[0, d], along(d))
+        send(ropes.at[0, 0], ropes.at[0, d], zs.at[1, d], zr.at[1, d], along(d))
+    send(latents.at[0, 0], latents.at[1, 0], ks.at[0, 0], kr.at[0, 0], partner)
+    send(ropes.at[0, 0], ropes.at[1, 0], ks.at[1, 0], kr.at[1, 0], partner)
+
+    second(1, order[1])
+    for d in range(planes):
+        arrived(metas.at[1, d], kr.at[2, d], partner)
+    spot = (
+        lax.broadcasted_iota(jnp.int32, (cap, PAD), 0)
+        == lax.broadcasted_iota(jnp.int32, (cap, PAD), 1)
+    ).astype(f32).astype(bf)
+    side_rows, side_slots = planes * cap, experts * planes * CAP
+    plane_of = jnp.concatenate(
+        [jnp.full((cap, 1), d, jnp.int32) for d in range(planes)], axis=0
+    )
+    slot_ids = lax.broadcasted_iota(jnp.int32, (side_rows, side_slots), 1)
+    for parity in range(2):
+        info = jnp.concatenate(
+            [
+                lax.dot_general(spot, metas[parity, d], across, preferred_element_type=f32)
+                for d in range(planes)
+            ],
+            axis=0,
+        )
+        info_b = info.astype(bf)
+        place = jnp.zeros((side_rows, side_slots), f32)
+        placed_t = jnp.zeros((side_slots, side_rows), f32)
+        slot_weights = jnp.zeros((side_slots, 1), f32)
+        for k in range(2):
+            column = info[:, k : k + 1]
+            code = column.astype(jnp.int32) - 1 - core * (experts * CAP)
+            inside = (column > 0.5) & (code >= 0) & (code < experts * CAP)
+            expert = jnp.zeros_like(code)
+            for e in range(1, experts):
+                expert += (code >= e * CAP).astype(jnp.int32)
+            where = expert * ((planes - 1) * CAP) + plane_of * CAP + code
+            match = (slot_ids == jnp.where(inside, where, -1)).astype(f32)
+            match_t = jnp.transpose(match)
+            place += match
+            placed_t += match_t
+            found = jnp.dot(match_t.astype(bf), info_b, preferred_element_type=f32)
+            slot_weights += found[:, 2 + k : 3 + k] + found[:, 4 + k : 5 + k]
+        place_v[parity] = place.astype(bf)
+        place_t[parity] = placed_t.astype(bf)
+        slot_w[parity] = slot_weights
+    feed(0)
+    fetch_down(2)
+    fetch_down(1)
+    second(1, order[-1])
+    for d in order[:-1]:
+        third(1, d)
+    for d in order:
+        first(0, d)
+    feed(1)
+    fetch_down(0)
+    third(1, order[-1])
+    for d in order[:-1]:
+        second(0, d)
+    feed(2)
+    second(0, order[-1])
+    feed(3)
+    def spread(s):
+        for piece in range(pieces):
+            down_in[s, piece].wait()
+        for e in range(experts):
+            act = both(hidden_v, e)
+            for piece in range(pieces):
+                cols = slice(piece * hidden, (piece + 1) * hidden)
+                result = jnp.dot(
+                    act, wbuf[down_slot[s], e, cols, :], preferred_element_type=f32
+                ).astype(bf)
+                for parity in range(2):
+                    given[parity, e * each : (e + 1) * each, cols] = result[
+                        parity * each : (parity + 1) * each
+                    ]
+        for parity in (1, 0):
+            summed = jnp.dot(place_v[parity], given[parity], preferred_element_type=f32).astype(bf)
+            part[s, parity] = summed.reshape(planes, cap, width)
+        for d in range(planes):
+            send(part.at[s, 1, d], other.at[s, d], cs.at[s, d], cr.at[s, d], partner)
+
+    def join(s, d):
+        arrived(other.at[s, d], cr.at[s, d], partner)
+        part[s, 0, d] = (part[s, 0, d].astype(f32) + other[s, d].astype(f32)).astype(bf)
+
+    def start(d):
+        send(part.at[3, 0, d, :, low], bx1.at[d], rs.at[0, d], rr.at[0, d], near_x)
+        send(part.at[3, 0, d, :, high], by1.at[d], rs.at[1, d], rr.at[1, d], near_y)
+
+    def rest_y(d):
+        send(part.at[2, 0, d, :, high], by2.at[d, :, high], rs.at[2, d], rr.at[2, d], near_y)
+
+    def rest_x(d):
+        send(part.at[1, 0, d, :, low], bx2.at[d, :, low], rs.at[3, d], rr.at[3, d], near_x)
+
+    def pass_on(d):
+        arrived(bx1.at[d], rr.at[0, d], near_x)
+        part[2, 0, d, :, low] = (
+            part[2, 0, d, :, low].astype(f32) + bx1[d].astype(f32)
+        ).astype(bf)
+        send(part.at[2, 0, d, :, low], by2.at[d, :, low], rs.at[4, d], rr.at[4, d], near_y)
+        arrived(by1.at[d], rr.at[1, d], near_y)
+        part[1, 0, d, :, high] = (
+            part[1, 0, d, :, high].astype(f32) + by1[d].astype(f32)
+        ).astype(bf)
+        send(part.at[1, 0, d, :, high], bx2.at[d, :, high], rs.at[5, d], rr.at[5, d], near_x)
+
+    def finish(d):
+        arrived(by2.at[d, :, high], rr.at[2, d], near_y)
+        arrived(bx2.at[d, :, low], rr.at[3, d], near_x)
+        arrived(by2.at[d, :, low], rr.at[4, d], near_y)
+        arrived(bx2.at[d, :, high], rr.at[5, d], near_x)
+        full = (
+            part[0, 0, d].astype(f32) + bx2[d].astype(f32) + by2[d].astype(f32)
+        ).astype(bf)
+        if d == 0:
+            back[0] = full
+        else:
+            done[d] = full
+            send(done.at[d], back.at[d], bs.at[d], br.at[d], along(-d))
+
+    spread(3)
+    for d in order:
+        third(0, d)
+    spread(2)
+    join(3, away[0])
+    start(away[0])
+    join(3, away[1])
+    start(away[1])
+    join(2, away[0])
+    rest_y(away[0])
+    for d in away[2:]:
+        join(3, d)
+    for d in away[1:]:
+        join(2, d)
+    spread(1)
+    join(1, away[0])
+    rest_x(away[0])
+    start(away[2])
+    for d in away[1:]:
+        join(1, d)
+    spread(0)
+    pass_on(away[0])
+    rest_y(away[1])
+    rest_x(away[1])
+    pass_on(away[1])
+    start(away[3])
+    rest_y(away[2])
+    rest_x(away[2])
+    for d in away:
+        join(0, d)
     for d in range(planes):
         arrived(latents.at[1, d], kr.at[0, d], partner)
         arrived(ropes.at[1, d], kr.at[1, d], partner)
@@ -594,7 +775,6 @@
     )
     key_t = key_t.astype(bf).astype(f32)
     values_v[...] = jnp.dot(key_rows, value_up_v[...], preferred_element_type=f32).astype(bf)
-    run_steps([(1, 1, 2), (2, 1, 1)])
     rope_t = jnp.concatenate(
         [ropes[parity, d].astype(f32) for parity in range(2) for d in range(planes)], axis=1
     )
@@ -629,163 +809,22 @@
         mixed_h = jnp.dot(expo.astype(bf), values_v[...], preferred_element_type=f32) / total
         return jnp.where(head_of == h, mixed_h, attn)
 
+    finish(away[0])
+    pass_on(away[2])
+    rest_y(away[3])
+    rest_x(away[3])
     attn = jnp.zeros((tokens, head_count * VDIM), f32)
     for h in range(head_count // 2):
         attn = attend(h, attn)
-    run_steps([(1, 1, 3)])
+    finish(away[1])
+    pass_on(away[3])
     for h in range(head_count // 2, head_count):
         attn = attend(h, attn)
     heads[tp] = attn.astype(bf)
-    run_steps([(2, 1, 2), (3, 1, 1)])
-
-    for d in range(planes):
-        arrived(metas.at[1, d], kr.at[2, d], partner)
-    spot = (
-        lax.broadcasted_iota(jnp.int32, (cap, PAD), 0)
-        == lax.broadcasted_iota(jnp.int32, (cap, PAD), 1)
-    ).astype(f32).astype(bf)
-    info = jnp.concatenate(
-        [
-            lax.dot_general(spot, metas[parity, d], across, preferred_element_type=f32)
-            for parity in range(2)
-            for d in range(planes)
-        ],
-        axis=0,
-    )
-    info_b = info.astype(bf)
-    block_of = jnp.concatenate(
-        [jnp.full((cap, 1), block, jnp.int32) for block in range(blocks)], axis=0
-    )
-    slot_ids = lax.broadcasted_iota(jnp.int32, (row_total, slot_total), 1)
-    place = jnp.zeros((row_total, slot_total), f32)
-    placed_t = jnp.zeros((slot_total, row_total), f32)
-    slot_weights = jnp.zeros((slot_total, 1), f32)
-    for k in range(2):
-        column = info[:, k : k + 1]
-        code = column.astype(jnp.int32) - 1 - core * (experts * CAP)
-        inside = (column > 0.5) & (code >= 0) & (code < experts * CAP)
-        expert = jnp.zeros_like(code)
-        for e in range(1, experts):
-            expert += (code >= e * CAP).astype(jnp.int32)
-        where = expert * (slots - CAP) + block_of * CAP + code
-        match = (slot_ids == jnp.where(inside, where, -1)).astype(f32)
-        match_t = jnp.transpose(match)
-        place += match
-        placed_t += match_t
-        found = jnp.dot(match_t.astype(bf), info_b, preferred_element_type=f32)
-        slot_weights += found[:, 2 + k : 3 + k] + found[:, 4 + k : 5 + k]
-    place_v[...] = place.astype(bf)
-    place_t[...] = placed_t.astype(bf)
-    slot_w[...] = slot_weights
-    run_steps([(2, 1, 3), (3, 1, 2)])
     for i, peer in enumerate((near_x, near_y, corner)):
         send(heads.at[tp], heads.at[tp], hs.at[i], hr.at[i], peer)
-
-    def feed(s):
-        for d in range(planes):
-            if s == 0 and d == 0:
-                arrived(rows_ref.at[:, 1, 0], pr.at[0, 0], partner)
-            elif d > 0:
-                arrived(rows_ref.at[tp ^ s, 1, d], pr.at[s, d], partner)
-        rows = rows_ref[tp ^ s].reshape(row_total, width)
-        taken[...] = jnp.dot(place_t[...], rows, preferred_element_type=f32).astype(bf)
-        gate_in[s].wait()
-        up_in[s].wait()
-        for e in range(experts):
-            mine = slice(e * slots, (e + 1) * slots)
-            picked = taken[mine, :]
-            gate = jnp.dot(picked, wbuf[s, e], preferred_element_type=f32)
-            upper = jnp.dot(picked, wbuf[4 + s, e], preferred_element_type=f32)
-            if s > 0:
-                gate += gate_acc[e]
-                upper += up_acc[e]
-            if s < 3:
-                gate_acc[e] = gate
-                up_acc[e] = upper
-            else:
-                hidden_v[mine, :] = (
-                    gate / (1.0 + jnp.exp(-gate)) * upper * slot_w[mine, :]
-                ).astype(bf)
-
-    feed(0)
-    fetch_down(2)
-    fetch_down(1)
-    run_steps([(3, 1, 3)])
-    feed(1)
-    fetch_down(0)
-    feed(2)
-    feed(3)
-
-    def spread(s):
-        for piece in range(pieces):
-            down_in[s, piece].wait()
-        for e in range(experts):
-            mine = slice(e * slots, (e + 1) * slots)
-            for piece in range(pieces):
-                cols = slice(piece * hidden, (piece + 1) * hidden)
-                given[mine, cols] = jnp.dot(
-                    hidden_v[mine, :], wbuf[down_slot[s], e, cols, :], preferred_element_type=f32
-                ).astype(bf)
-        summed = jnp.dot(place_v[...], given[...], preferred_element_type=f32).astype(bf)
-        part[s] = summed.reshape(2, planes, cap, width)
-        for d in range(planes):
-            send(part.at[s, 1, d], other.at[s, d], cs.at[s, d], cr.at[s, d], partner)
-
-    def join(s):
-        for d in range(planes):
-            arrived(other.at[s, d], cr.at[s, d], partner)
-            part[s, 0, d] = (part[s, 0, d].astype(f32) + other[s, d].astype(f32)).astype(bf)
-
-    away = order + [0]
-
-    def start_rest(d):
-        send(part.at[2, 0, d, :, high], by2.at[d, :, high], rs.at[2, d], rr.at[2, d], near_y)
-        send(part.at[1, 0, d, :, low], bx2.at[d, :, low], rs.at[3, d], rr.at[3, d], near_x)
-
-    def pass_on(d):
-        arrived(bx1.at[d], rr.at[0, d], near_x)
-        part[2, 0, d, :, low] = (
-            part[2, 0, d, :, low].astype(f32) + bx1[d].astype(f32)
-        ).astype(bf)
-        send(part.at[2, 0, d, :, low], by2.at[d, :, low], rs.at[4, d], rr.at[4, d], near_y)
-        arrived(by1.at[d], rr.at[1, d], near_y)
-        part[1, 0, d, :, high] = (
-            part[1, 0, d, :, high].astype(f32) + by1[d].astype(f32)
-        ).astype(bf)
-        send(part.at[1, 0, d, :, high], bx2.at[d, :, high], rs.at[5, d], rr.at[5, d], near_x)
-
-    def finish(d):
-        arrived(by2.at[d, :, high], rr.at[2, d], near_y)
-        arrived(bx2.at[d, :, low], rr.at[3, d], near_x)
-        arrived(by2.at[d, :, low], rr.at[4, d], near_y)
-        arrived(bx2.at[d, :, high], rr.at[5, d], near_x)
-        full = (
-            part[0, 0, d].astype(f32) + bx2[d].astype(f32) + by2[d].astype(f32)
-        ).astype(bf)
-        if d == 0:
-            back[0] = full
-        else:
-            done[d] = full
-            send(done.at[d], back.at[d], bs.at[d], br.at[d], along(-d))
-
-    spread(3)
-    spread(2)
-    join(3)
-    for d in away:
-        send(part.at[3, 0, d, :, low], bx1.at[d], rs.at[0, d], rr.at[0, d], near_x)
-        send(part.at[3, 0, d, :, high], by1.at[d], rs.at[1, d], rr.at[1, d], near_y)
-    spread(1)
-    join(2)
-    join(1)
-    for d in order:
-        start_rest(d)
-    spread(0)
-    for d in order:
-        pass_on(d)
-    start_rest(0)
-    pass_on(0)
-    join(0)
-
+    finish(away[2])
+    finish(away[3])
     for i, peer in enumerate((near_x, near_y, corner)):
         arrived(heads.at[tp ^ (i + 1)], hr.at[i], peer)
     loads["out_gain"].wait()
@@ -796,8 +835,6 @@
     product = jnp.dot(scaled, out_proj_v[...], preferred_element_type=f32)
     mixed_ref[...] = (product * lax.rsqrt(squares + EPS)).astype(bf)
 
-    for d in away:
-        finish(d)
     for d in order:
         arrived(back.at[d], br.at[d], along(d))
     expert_ref[...] = jnp.dot(
@@ -865,8 +902,8 @@
     mixed, expert_out = pl.pallas_call(
         functools.partial(layer_kernel, planes),
         out_shape=(
-            jax.ShapeDtypeStruct((tokens, out_proj.shape[1]), bf),
-            jax.ShapeDtypeStruct((tokens, width), bf),
+            pltpu.VMEM((tokens, out_proj.shape[1]), bf),
+            pltpu.VMEM((tokens, width), bf),
         ),
         in_specs=[pl.BlockSpec(memory_space=pl.ANY)] * len(operands),
         out_specs=(pl.BlockSpec(memory_space=pltpu.VMEM),) * 2,
@@ -897,14 +934,14 @@
             vmem((total, v_cols), bf),
             vmem((4, tokens, v_cols), bf),
             vmem((tokens, planes * cap), bf),
-            vmem((row_total, slot_total), bf),
-            vmem((slot_total, row_total), bf),
-            vmem((slot_total, 1), f32),
-            vmem((slot_total, width), bf),
+            vmem((2, row_total // 2, slot_total // 2), bf),
+            vmem((2, slot_total // 2, row_total // 2), bf),
+            vmem((2, slot_total // 2, 1), f32),
+            vmem((2, slot_total // 2, width), bf),
             vmem((experts, slots, hidden), f32),
             vmem((experts, slots, hidden), f32),
-            vmem((slot_total, hidden), bf),
-            vmem((slot_total, width), bf),
+            vmem((2, slot_total // 2, hidden), bf),
+            vmem((2, slot_total // 2, width), bf),
             vmem((4, 2, planes, cap, width), bf),
             vmem((4, planes, cap, width), bf),
             vmem((planes, cap, width // 2), bf),
@@ -933,11 +970,39 @@
             dma((planes,)),
         ],
         compiler_params=pltpu.CompilerParams(
-            collective_id=0, has_side_effects=True, vmem_limit_bytes=67043328
+            collective_id=0, has_side_effects=True, vmem_limit_bytes=62 * 2**20
         ),
         name="layer",
     )(*operands)
-    return (mixed, expert_out)
+    return flush(mixed, expert_out)
+
+
+def flush_kernel(a_ref, b_ref, x_ref, y_ref, sems):
+    copies = [
+        pltpu.make_async_copy(a_ref, x_ref, sems.at[0]),
+        pltpu.make_async_copy(b_ref, y_ref, sems.at[1]),
+    ]
+    for copy in copies:
+        copy.start()
+    for copy in copies:
+        copy.wait()
+
+
+def flush(first_out, second_out):
+    return pl.pallas_call(
+        flush_kernel,
+        out_shape=(
+            jax.ShapeDtypeStruct(first_out.shape, first_out.dtype),
+            jax.ShapeDtypeStruct(second_out.shape, second_out.dtype),
+        ),
+        in_specs=[pl.BlockSpec(memory_space=pltpu.VMEM)] * 2,
+        out_specs=(pl.BlockSpec(memory_space=pl.ANY),) * 2,
+        scratch_shapes=[pltpu.SemaphoreType.DMA((2,))],
+        name="flush",
+    )(
+        pltpu.with_memory_space_constraint(first_out, pltpu.VMEM),
+        pltpu.with_memory_space_constraint(second_out, pltpu.VMEM),
+    )
 
 
 def layer(*arrays):
@@ -945,8 +1010,7 @@
     tp_count, ep_count = lax.axis_size("tp"), lax.axis_size("ep")
     fits = (
         tp_count == 4
-        and ep_count % 2 == 0
-        and ep_count // 2 <= GROUP
+        and ep_count == 2 * tp_count
         and 2 * gate.shape[0] == GROUP
         and stream.shape[0] == PAD
         and stream.shape[1] // tp_count == 2 * gate.shape[2]

time: 72.1 us -> 56.1 us (0.78)
  Pallas kernels: 67.9 us -> 55.2 us
  local copies, waits for them, and re-layouts: 3.34 us -> 0 us
    pallas_call x1 -> x2, Pallas kernels: 67.9 us -> 55.2 us  [the longest x1 54.4 us: fused(): pl.pallas_call(functools.partial(layer_kernel, planes), out_shape=(pltpu....]
    unnamed x2 -> x0, local copies, waits for them, and re-layouts: 3.34 us -> none
where the time goes in v2:
time: 56.1 us; the launch traced here: 56 us
  Pallas kernels  55.2 us (98%)
  between operations  0.81 us (1%)
    pallas_call x1, Pallas kernels, fused(): pl.pallas_call(functools.partial(layer_kernel, planes), out_shape=(pltpu....  54.4 us

profile of v2, /device:TPU:0, one launch (start us, length us, event | category | flops | bytes accessed | tf_op | source)
XLA Modules:
  0.0 56.0 jit_solution(8646000731159505094)
XLA Ops:
  0.6 54.4 %layer.1 = (bf16[128,1024]{1,0:T(8,128)(2,1)S(1)}, bf16[128,1024]{1,0:T(8,128)(2,1)S(1)}) custom-call(bf16[128,384]{1,0:T(8,128)(2,1)} %queries_in.1, bf16[128,512]{1,0:T(8,128)(2,1)} %latent_in.1, bf16[32,128]{1,0:T(8,128)(2,1)} %bitcast.9, f32[1,512]{1,0:T(1,128)} %bitcast.11, bf16[512,256]{1,0:T(8,128)(2,1)} %key_up_in.1, bf16[512,256]{1,0:T(8,128)(2,1)} %value_up_in.1, ...), custom_call_target="tpu_custom_call" | custom-call | tf_op jit(solution)/shard_map/layer/pallas_call | solution.py:902
  55.0 0.8 %flush.1 = (bf16[128,1024]{1,0:T(8,128)(2,1)}, bf16[128,1024]{1,0:T(8,128)(2,1)}) custom-call(bf16[128,1024]{1,0:T(8,128)(2,1)S(1)} %get-tuple-element.4.a_ref, bf16[128,1024]{1,0:T(8,128)(2,1)S(1)} %get-tuple-element.5.b_ref), custom_call_target="tpu_custom_call" | custom-call | tf_op jit(solution)/shard_map/flush/pallas_call | solution.py:992

commit v3 on v2

--- a/solution.py
+++ b/solution.py
@@ -224,13 +224,6 @@
     near_y = (ep, tp ^ 2)
     corner = (ep, tp ^ 3)
     return tp, along, partner, near_x, near_y, corner
-
-
-def greet(peers):
-    barrier = pltpu.get_barrier_semaphore()
-    for peer in peers:
-        pl.semaphore_signal(barrier, inc=1, device_id=peer, device_id_type=MESH)
-    pl.semaphore_wait(barrier, len(peers))
 
 
 def rope_table(total):
@@ -475,8 +468,9 @@
         outgoing[d] = out_rows[(d - 1) * cap : d * cap]
     pl.semaphore_wait(barrier, len(peers))
     for d in order:
+        send(metas_out.at[d], metas.at[0, d], zs.at[2, d], zr.at[2, d], along(d))
+    for d in order:
         send(outgoing.at[d], rows_ref.at[tp, 0, d], zs.at[3, d], zr.at[3, d], along(d))
-        send(metas_out.at[d], metas.at[0, d], zs.at[2, d], zr.at[2, d], along(d))
     for q in range(4):
         cols = slice(q * width, (q + 1) * width)
         normed_q = (stream_v[:, cols].astype(f32) * scale * moe_gain_v[:, cols]).astype(bf)
@@ -508,8 +502,6 @@
             send(ropes.at[0, d], ropes.at[1, d], ks.at[1, d], kr.at[1, d], partner)
         else:
             send(mine, rows_ref.at[tp, 1, d], ps.at[0, d], pr.at[0, d], partner)
-            arrived(metas.at[0, d], zr.at[2, d], along(-d))
-            send(metas.at[0, d], metas.at[1, d], ks.at[2, d], kr.at[2, d], partner)
 
     def half_of(kind, flip, d, side):
         if kind == 0:
@@ -600,20 +592,9 @@
                         parity * each : (parity + 1) * each
                     ]
 
-    first(1, order[0])
-    first(1, order[1])
-    second(1, order[0])
-    first(1, order[2])
-    own_part = latents.at[0, 0, quarter(tp)]
     for d in order:
-        send(own_part, latents.at[0, d, quarter(tp)], zs.at[0, d], zr.at[0, d], along(d))
-        send(ropes.at[0, 0], ropes.at[0, d], zs.at[1, d], zr.at[1, d], along(d))
-    send(latents.at[0, 0], latents.at[1, 0], ks.at[0, 0], kr.at[0, 0], partner)
-    send(ropes.at[0, 0], ropes.at[1, 0], ks.at[1, 0], kr.at[1, 0], partner)
-
-    second(1, order[1])
-    for d in range(planes):
-        arrived(metas.at[1, d], kr.at[2, d], partner)
+        arrived(metas.at[0, d], zr.at[2, d], along(-d))
+        send(metas.at[0, d], metas.at[1, d], ks.at[2, d], kr.at[2, d], partner)
     spot = (
         lax.broadcasted_iota(jnp.int32, (cap, PAD), 0)
         == lax.broadcasted_iota(jnp.int32, (cap, PAD), 1)
@@ -623,7 +604,7 @@
         [jnp.full((cap, 1), d, jnp.int32) for d in range(planes)], axis=0
     )
     slot_ids = lax.broadcasted_iota(jnp.int32, (side_rows, side_slots), 1)
-    for parity in range(2):
+    def settle(parity):
         info = jnp.concatenate(
             [
                 lax.dot_general(spot, metas[parity, d], across, preferred_element_type=f32)
@@ -652,6 +633,23 @@
         place_v[parity] = place.astype(bf)
         place_t[parity] = placed_t.astype(bf)
         slot_w[parity] = slot_weights
+
+    settle(0)
+    first(1, order[0])
+    for d in range(planes):
+        arrived(metas.at[1, d], kr.at[2, d], partner)
+    settle(1)
+    first(1, order[1])
+    second(1, order[0])
+    first(1, order[2])
+    own_part = latents.at[0, 0, quarter(tp)]
+    for d in order:
+        send(own_part, latents.at[0, d, quarter(tp)], zs.at[0, d], zr.at[0, d], along(d))
+        send(ropes.at[0, 0], ropes.at[0, d], zs.at[1, d], zr.at[1, d], along(d))
+    send(latents.at[0, 0], latents.at[1, 0], ks.at[0, 0], kr.at[0, 0], partner)
+    send(ropes.at[0, 0], ropes.at[1, 0], ks.at[1, 0], kr.at[1, 0], partner)
+
+    second(1, order[1])
     feed(0)
     fetch_down(2)
     fetch_down(1)
@@ -685,7 +683,7 @@
         for parity in (1, 0):
             summed = jnp.dot(place_v[parity], given[parity], preferred_element_type=f32).astype(bf)
             part[s, parity] = summed.reshape(planes, cap, width)
-        for d in range(planes):
+        for d in away:
             send(part.at[s, 1, d], other.at[s, d], cs.at[s, d], cr.at[s, d], partner)
 
     def join(s, d):
@@ -729,9 +727,8 @@
             send(done.at[d], back.at[d], bs.at[d], br.at[d], along(-d))
 
     spread(3)
-    for d in order:
-        third(0, d)
     spread(2)
+    spread(1)
     join(3, away[0])
     start(away[0])
     join(3, away[1])
@@ -742,7 +739,8 @@
         join(3, d)
     for d in away[1:]:
         join(2, d)
-    spread(1)
+    for d in order:
+        third(0, d)
     join(1, away[0])
     rest_x(away[0])
     start(away[2])

time: 56.1 us -> 54.3 us (0.968)
  Pallas kernels: 55.2 us -> 53.3 us
    pallas_call x1, Pallas kernels: 54.4 us -> 52.5 us  [fused(): pl.pallas_call(functools.partial(layer_kernel, planes), out_shape=(pltpu....]
where the time goes in v3:
time: 54.3 us; the launch traced here: 54.1 us
  Pallas kernels  53.3 us (98%)
  between operations  0.81 us (1%)
    pallas_call x1, Pallas kernels, fused(): pl.pallas_call(functools.partial(layer_kernel, planes), out_shape=(pltpu....  52.5 us

profile of v3, /device:TPU:0, one launch (start us, length us, event | category | flops | bytes accessed | tf_op | source)
XLA Modules:
  0.0 54.1 jit_solution(788761943383671467)
XLA Ops:
  0.6 52.5 %layer.1 = (bf16[128,1024]{1,0:T(8,128)(2,1)S(1)}, bf16[128,1024]{1,0:T(8,128)(2,1)S(1)}) custom-call(bf16[128,384]{1,0:T(8,128)(2,1)} %queries_in.1, bf16[128,512]{1,0:T(8,128)(2,1)} %latent_in.1, bf16[32,128]{1,0:T(8,128)(2,1)} %bitcast.9, f32[1,512]{1,0:T(1,128)} %bitcast.11, bf16[512,256]{1,0:T(8,128)(2,1)} %key_up_in.1, bf16[512,256]{1,0:T(8,128)(2,1)} %value_up_in.1, ...), custom_call_target="tpu_custom_call" | custom-call | tf_op jit(solution)/shard_map/layer/pallas_call | solution.py:900
  53.1 0.8 %flush.1 = (bf16[128,1024]{1,0:T(8,128)(2,1)}, bf16[128,1024]{1,0:T(8,128)(2,1)}) custom-call(bf16[128,1024]{1,0:T(8,128)(2,1)S(1)} %get-tuple-element.4.a_ref, bf16[128,1024]{1,0:T(8,128)(2,1)S(1)} %get-tuple-element.5.b_ref), custom_call_target="tpu_custom_call" | custom-call | tf_op jit(solution)/shard_map/flush/pallas_call | solution.py:990
